TPU v7x, 128 devices: a whole 4x4x4 slice. The times are simulated.
128 devices in a mesh: sp: 64 (over z, y, x), tp: 2 (over core).
Axes of the slice: x: 4, y: 4, z: 4, core: 2. Of those that a mesh axis runs over, the one named last changes fastest.
Arguments:
- features: bfloat16 [32768, 4096], P('sp', 'tp'), may hold values from -16 to 16
- weight_value: bfloat16 [4096, 1024], P(None, 'tp'), may hold values from -0.09375 to 0.09375
- weight_gate: bfloat16 [4096, 1024], P(None, 'tp'), may hold values from -0.09375 to 0.09375
- weight_out: bfloat16 [4096, 1024], P(None, 'tp'), may hold values from -0.1875 to 0.1875
- conv_taps: float32 [31, 1024], P(None, 'tp'), may hold values from -6 to 6
- norm_gain: float32 [1024], P('tp'), may hold values from 0.1 to 1.9
- out_grad: bfloat16 [32768, 4096], P('sp', 'tp'), may hold values from -16 to 16
Outputs:
- value_grad: float32 [32768, 1024], P('sp', 'tp')
- gate_grad: float32 [32768, 1024], P('sp', 'tp')
- value_wgrad: float32 [4096, 1024], P('sp', 'tp')
- gate_wgrad: float32 [4096, 1024], P('sp', 'tp')
- out_wgrad: float32 [4096, 1024], P('sp', 'tp')
- taps_grad: float32 [31, 1024], P(None, 'tp')
- gain_grad: float32 [1024], P('tp')
All inputs are finite; a program needn't handle non-finite values.
Results may differ from a plain program's by a relative error of at most 0.0057.
Values may be sent and summed in bfloat16 or wider, within the bound.
A program may use at most 192 MiB of HBM per device.

v0:
```python
import jax
import jax.numpy as jnp
from jax import lax
from jax.sharding import Mesh
from jax.sharding import PartitionSpec as P

SP = ("sp_0", "sp_1", "sp_2")


NORM_EPS = 1e-05


def sum_by_axis(running, axes):
    for axis in axes:
        running = lax.psum_scatter(running, axis, scatter_dimension=0, tiled=True)
    return running


def in_one_piece(arrays, axis, dim, along):
    ends, at = ([], 0)
    for a in arrays[:-1]:
        at += a.shape[along]
        ends.append(at)
    both = jnp.concatenate(arrays, axis=along)
    return tuple(jnp.split(lax.all_gather(both, axis, axis=dim, tiled=True), ends, axis=along))


def with_halo(block, sides, width):
    for axis, dim in sides:
        count = lax.axis_size(axis)
        forward = [(i, i + 1) for i in range(count - 1)]
        backward = [(target, source) for source, target in forward]
        low = lax.ppermute(
            lax.slice_in_dim(block, block.shape[dim] - width, None, axis=dim), axis, forward
        )
        high = lax.ppermute(lax.slice_in_dim(block, 0, width, axis=dim), axis, backward)
        block = jnp.concatenate([low, block, high], axis=dim)
    return block


def from_everyone(x, axis):
    devices = lax.axis_size(axis)
    return lax.all_to_all(jnp.broadcast_to(x[None], (devices, *x.shape)), axis, 0, 0, tiled=True)


def of_everyone(x, axis):
    return from_everyone(x, axis).sum(axis=0)


def packed_total(arrays, axis):
    vector, at, finished = (jnp.concatenate([a.reshape(-1) for a in arrays]), 0, [])
    running = of_everyone(vector, axis)
    for a in arrays:
        finished.append(running[at : at + a.size].reshape(a.shape))
        at += a.size
    return tuple(finished)


def total_of_pieces(x, axis):
    return lax.all_gather(x, axis).sum(0)


def make_term(left_rows, right_rows):
    return lax.dot_general(
        left_rows, right_rows, (((0,), (0,)), ((), ())), preferred_element_type=jnp.float32
    )


def out_weight_sum(whole_cotangent, act_half):
    return sum_by_axis(make_term(whole_cotangent, act_half), SP)


def on_device(features, weight_value, weight_gate, weight_out, conv_taps, norm_gain, out_grad):
    whole_inputs, whole_cotangent = in_one_piece((features, out_grad), "tp", 1, 0)
    value_half = jnp.dot(whole_inputs, weight_value, preferred_element_type=jnp.float32).astype(
        jnp.bfloat16
    )
    gate_half = jnp.dot(whole_inputs, weight_gate, preferred_element_type=jnp.float32).astype(
        jnp.bfloat16
    )
    value_half, gate_half = lax.optimization_barrier((value_half, gate_half))
    value_pre = value_half.astype(jnp.float32)
    gate_pre = gate_half.astype(jnp.float32)
    gate_sig = jax.nn.sigmoid(gate_pre)
    mixed_half = lax.optimization_barrier((value_pre * gate_sig).astype(jnp.bfloat16))
    tap_count = conv_taps.shape[0]
    half_width = tap_count // 2
    row_count = mixed_half.shape[0]
    channels = mixed_half.shape[1] * lax.axis_size("tp")
    extended = with_halo(mixed_half, ((SP, 0),), half_width).astype(jnp.float32)
    conv_out = jnp.zeros(mixed_half.shape, jnp.float32)
    for offset in range(tap_count):
        conv_out = conv_out + conv_taps[offset] * extended[offset : offset + row_count]
    row_sum, row_square = packed_total(
        (jnp.sum(conv_out, axis=-1), jnp.sum(conv_out * conv_out, axis=-1)), "tp"
    )
    mean_row = row_sum[:, None] / channels
    var_row = row_square[:, None] / channels - mean_row * mean_row
    inv_std = lax.rsqrt(var_row + NORM_EPS)
    normed = (conv_out - mean_row) * inv_std
    pre_act = normed * norm_gain
    act_sig = jax.nn.sigmoid(pre_act)
    act_half = (pre_act * act_sig).astype(jnp.bfloat16)
    act_grad = jnp.dot(whole_cotangent, weight_out, preferred_element_type=jnp.float32)
    pre_grad = act_grad * act_sig * (1.0 + pre_act * (1.0 - act_sig))
    gain_part = jnp.sum(pre_grad * normed, axis=0)
    norm_grad = pre_grad * norm_gain
    first_sum, second_sum = packed_total(
        (jnp.sum(norm_grad, axis=-1), jnp.sum(norm_grad * normed, axis=-1)), "tp"
    )
    first_mom = first_sum[:, None] / channels
    second_mom = second_sum[:, None] / channels
    conv_grad = inv_std * (norm_grad - first_mom - normed * second_mom)
    grad_ext = with_halo(conv_grad, ((SP, 0),), half_width)
    mixed_grad = jnp.zeros(conv_grad.shape, jnp.float32)
    taps_rows = []
    for offset in range(tap_count):
        begin = 2 * half_width - offset
        mixed_grad = mixed_grad + conv_taps[offset] * grad_ext[begin : begin + row_count]
        taps_rows.append(jnp.sum(conv_grad * extended[offset : offset + row_count], axis=0))
    taps_grad, gain_grad = (
        total_of_pieces(jnp.stack(taps_rows), SP),
        total_of_pieces(gain_part, SP),
    )
    value_grad = mixed_grad * gate_sig
    gate_grad = mixed_grad * value_pre * gate_sig * (1.0 - gate_sig)
    value_low = value_grad.astype(jnp.bfloat16)
    gate_low = gate_grad.astype(jnp.bfloat16)
    out_wgrad = out_weight_sum(whole_cotangent, act_half)
    both_low = jnp.concatenate([value_low, gate_low], axis=1)
    joined = lax.psum_scatter(
        make_term(whole_inputs, both_low), SP, scatter_dimension=0, tiled=True
    )
    split_at = value_low.shape[1]
    value_wgrad = joined[:, :split_at]
    gate_wgrad = joined[:, split_at:]
    return (value_grad, gate_grad, value_wgrad, gate_wgrad, out_wgrad, taps_grad, gain_grad)


def solution(mesh):
    split = Mesh(mesh.devices.reshape(4, 4, 4, mesh.shape["tp"]), ("sp_0", "sp_1", "sp_2", "tp"))
    return jax.shard_map(
        on_device,
        mesh=split,
        in_specs=(
            P(SP, "tp"),
            P(None, "tp"),
            P(None, "tp"),
            P(None, "tp"),
            P(None, "tp"),
            P("tp"),
            P(SP, "tp"),
        ),
        out_specs=(
            P(SP, "tp"),
            P(SP, "tp"),
            P(SP, "tp"),
            P(SP, "tp"),
            P(SP, "tp"),
            P(None, "tp"),
            P("tp"),
        ),
        check_vma=False,
    )
```

profile of v0, /device:TPU:0, one launch (start us, length us, event | category | flops | bytes accessed | tf_op | source)
XLA Modules:
  0.0 679.9 jit_solution(18109533165269023774)
XLA Ops:
  7.2 0.0 all-gather.7.cloned.1.call-start
  7.2 4.7 pad_maximum_fusion
  11.9 0.0 copy-start.1
  12.0 0.0 all-gather.7.cloned.1.call-update
  12.0 0.0 reduce-scatter.7.cloned.1.call-start
  12.0 0.8 copy-done.1
  12.8 24.3 %all-gather.7.cloned.1.call-done = bf16[1024,4096]{1,0:T(8,128)(2,1)} async-done(((bf16[1024,2048]{1,0:T(8,128)(2,1)}), bf16[1024,4096]{1,0:T(8,128)(2,1)}) %all-gather.7.cloned.1.call-update) | async-done | bytes 8388624 | tf_op jit(solution)/shard_map/all_gather | solution.py:25
  37.2 0.0 copy-start.3
  37.2 0.0 copy-start.4
  37.2 5.9 fusion.19
  43.1 0.0 copy-done.3
  43.1 1.1 copy-done.4
  44.2 2.3 fusion.16
  46.5 0.3 fusion.22
  46.8 3.5 collective-permute-start
  50.3 1.3 collective-permute-start.1
  51.6 0.1 collective-permute-done
  51.7 4.2 collective-permute-done.1
  55.9 0.2 maximum_convert_fusion
  56.1 0.0 copy-start.2
  56.1 5.0 fusion.123
  61.2 0.0 copy-start
  61.2 3.7 all_to_all.12
  64.9 0.0 copy-done.2
  65.0 8.0 %fusion = f32[4096,512]{1,0:T(8,128)} fusion(bf16[1024,4096]{1,0:T(8,128)(2,1)} %all-gather.7.cloned.1.call-done, f32[512,512]{1,0:T(8,128)S(1)} %get-tuple-element.53, f32[512]{0:T(512)S(1)} %copy-done.2, f32[512]{0:T(512)S(1)} %get-tuple-element.94, f32[512]{0:T(512)S(1)} %get-tuple-element.93), kind=kOutput, calls=%fused_computation.29 | convolution fusion | flops 2149580800 | bytes 13637632 | tf_op jit(solution)/shard_map/dot_general | solution.py:64
  72.9 0.0 reduce-scatter.7.cloned.1.call-update
  73.0 0.0 reduce-scatter.9.cloned.1.call-start
  73.0 85.5 %reduce-scatter.7.cloned.1.call-done = f32[1024,512]{1,0:T(8,128)} async-done(((f32[4096,512]{1,0:T(8,128)}), f32[1024,512]{1,0:T(8,128)}) %reduce-scatter.7.cloned.1.call-update) | async-done | bytes 2097168 | tf_op jit(solution)/shard_map/reduce_scatter | solution.py:15
  158.5 0.0 reduce-scatter.9.cloned.1.call-update
  158.5 0.0 all-gather.9.cloned.1.call-start
  158.6 0.0 copy-done
  158.6 7.1 %multiply_reduce_fusion = (f32[512]{0:T(512)S(1)}, f32[512]{0:T(512)S(1)}, f32[512]{0:T(512)S(1)}, f32[512,512]{1,0:T(8,128)}) fusion(f32[512,512]{1,0:T(8,128)S(1)} %get-tuple-element.53, f32[512]{0:T(512)S(1)} %get-tuple-element.94, f32[512]{0:T(512)S(1)} %get-tuple-element.93, f32[512]{0:T(512)S(1)} %copy-done.2, bf16[4096,512]{1,0:T(8,128)(2,1)} %param.10, ...), kind=kOutput, calls=%fused_computation.164 | convolution fusion | flops 2151938560 | bytes 10498048 | tf_op jit(solution)/shard_map/dot_general | solution.py:104
  165.8 3.7 all_to_all.13
  169.5 4.2 multiply_reduce_fusion.1
  173.7 1.7 multiply_reduce_fusion.2
  175.4 2.5 stack.127
  178.0 0.0 all-gather.9.cloned.1.call-update
  178.0 0.0 reduce-scatter.5.cloned.1.call-start
  178.1 1.3 collective-permute-start.2
  179.4 4.5 collective-permute-start.3
  183.9 0.0 collective-permute-done.2
  183.9 1.6 collective-permute-done.3
  185.5 5.6 fusion.124
  191.2 1.3 fusion.127
  192.5 12.6 %fusion.4 = f32[4096,1024]{1,0:T(8,128)} fusion(bf16[1024,4096]{1,0:T(8,128)(2,1)} %all-gather.7.cloned.1.call-done, bf16[512,512]{1,0:T(8,128)(2,1)S(1)} %get-tuple-element.51, bf16[512,512]{1,0:T(8,128)(2,1)} %get-tuple-element.48), kind=kOutput, calls=%fused_computation.33 | convolution fusion | flops 4297064448 | bytes 22020096 | tf_op jit(solution)/shard_map/dot_general | solution.py:64
  205.1 0.0 reduce-scatter.5.cloned.1.call-update
  205.1 0.0 reduce-scatter.11.cloned.1.call-start
  205.2 0.0 reduce-scatter.9.cloned.1.call-done
  205.2 0.5 reduce-scatter.11.cloned.1.call-update
  205.7 176.6 %all-gather.3 = f32[64,1,512]{2,1,0:T(1,128)S(1)} all-gather(f32[1,1,512]{2,1,0:T(1,128)S(1)} %bitcast.161), channel_id=3, replica_groups=mesh['sp_0'=4,'sp_1'=4,'sp_2'=4,'tp'=2] {'sp_0','sp_1','sp_2'}, dimensions={0}, use_global_device_ids=true | all-gather | bytes 133120 | tf_op jit(solution)/shard_map/all_gather | solution.py:60
  382.3 0.7 reduce_sum.399
  382.9 0.0 all-gather.9.cloned.1.call-done
  383.0 3.2 reduce_sum.397
  386.1 267.2 %reduce-scatter.5.cloned.1.call-done = f32[64,1024]{1,0:T(8,128)} async-done(((f32[4096,1024]{1,0:T(8,128)}), f32[64,1024]{1,0:T(8,128)}) %reduce-scatter.5.cloned.1.call-update) | async-done | bytes 262160 | tf_op jit(solution)/shard_map/reduce_scatter | solution.py:131
  653.3 1.7 fusion.131
  655.0 18.1 %reduce-scatter.11.cloned.1.call-done = f32[64,512]{1,0:T(8,128)} async-done(((f32[256,512]{1,0:T(8,128)}), f32[64,512]{1,0:T(8,128)}) %reduce-scatter.11.cloned.1.call-update) | async-done | bytes 131088 | tf_op jit(solution)/shard_map/reduce_scatter | solution.py:15
  (12 shorter events, 0.1 us)
Async XLA Ops:
  7.2 30.0 %all-gather.7.cloned.1.call-start = ((), (), s32[]{:S(2)}) async-start(), calls=%async_computation.6 | async-start | bytes 12582912 | tf_op jit(solution)/shard_map/all_gather | solution.py:25
  11.9 0.8 copy-start.1
  12.0 146.5 %reduce-scatter.7.cloned.1.call-start = ((), (), s32[]{:S(2)}) async-start(), calls=%async_computation.8 | async-start | bytes 10485760 | tf_op jit(solution)/shard_map/reduce_scatter | solution.py:15
  37.2 5.9 copy-start.3
  37.2 7.0 %copy-start.4 = (bf16[4096,512]{1,0:T(8,128)(2,1)S(1)}, bf16[4096,512]{1,0:T(8,128)(2,1)}, u32[]{:S(2)}) copy-start(bf16[4096,512]{1,0:T(8,128)(2,1)} %param.8) | copy-start | bytes 12582916
  46.8 4.9 collective-permute-start
  50.3 5.6 collective-permute-start.1
  56.1 8.9 %copy-start.2 = (f32[512]{0:T(512)S(1)}, f32[512]{0:T(512)}, u32[]{:S(2)}) copy-start(f32[512]{0:T(512)} %param.12) | copy-start | bytes 6148
  61.2 97.4 %copy-start = (f32[512,512]{1,0:T(8,128)}, f32[512,512]{1,0:T(8,128)S(1)}, u32[]{:S(2)}) copy-start(f32[512,512]{1,0:T(8,128)S(1)} %get-tuple-element.53) | copy-start | bytes 3145732
  73.0 132.2 %reduce-scatter.9.cloned.1.call-start = ((), (), s32[]{:S(2)}) async-start(), calls=%async_computation.9 | async-start | bytes 2621440 | tf_op jit(solution)/shard_map/reduce_scatter | solution.py:15
  158.5 224.4 %all-gather.9.cloned.1.call-start = ((), (), s32[]{:S(2)}) async-start(), calls=%async_computation.11 | async-start | bytes 4259840 | tf_op jit(solution)/shard_map/all_gather | solution.py:60
  178.0 475.3 %reduce-scatter.5.cloned.1.call-start = ((), (), s32[]{:S(2)}) async-start(), calls=%async_computation.7 | async-start | bytes 17039360 | tf_op jit(solution)/shard_map/reduce_scatter | solution.py:131
  178.1 5.9 collective-permute-start.2
  179.4 6.1 collective-permute-start.3
  205.1 468.0 %reduce-scatter.11.cloned.1.call-start = ((), (), s32[]{:S(2)}) async-start(), calls=%async_computation.10 | async-start | bytes 655360 | tf_op jit(solution)/shard_map/reduce_scatter | solution.py:15
Sparse Core Ops, SparseCore 0:
  12.1 25.0 all-gather.6
  73.1 85.3 reduce-scatter.6
  160.9 29.2 reduce-scatter.8
  193.5 68.7 all-gather.8
  264.6 388.7 reduce-scatter.4
  656.2 16.8 reduce-scatter.10
where the time goes:
time: 680 us
  waiting for transfers between devices  402 us (59%)
  blocking collectives  184 us (27%)
  matrix products  36 us (5%)
  other arithmetic  27 us (4%)
  between operations  14.3 us (2%)
  starting transfers between devices  10.8 us (2%)
    reduce_scatter x1, waiting for transfers between devices, on_device(): lax.psum_scatter(make_term(whole_inputs, both_low), SP, scatter_dimension...  267 us
    all_gather x1, blocking collectives, total_of_pieces(): return lax.all_gather(x, axis).sum(0)  177 us
    reduce_scatter x3, waiting for transfers between devices, sum_by_axis(): running = lax.psum_scatter(running, axis, scatter_dimension=0, tiled=True)  104 us
    all_gather x1, waiting for transfers between devices, in_one_piece(): lax.all_gather(both, axis, axis=dim, tiled=True)  24.3 us
    dot_general x2, matrix products, make_term(): lax.dot_general(left_rows, right_rows, (((0,), (0,)), ((), ())), preferre...  20.6 us
  transfers between devices with their start and end apart: 10, of which 7 were waited for; matrix products, arithmetic and copies ran while one was open for 6% of the time, Pallas kernels for 0%

commit v1 on v0

--- a/solution.py
+++ b/solution.py
@@ -67,7 +67,8 @@
 
 
 def out_weight_sum(whole_cotangent, act_half):
-    return sum_by_axis(make_term(whole_cotangent, act_half), SP)
+    term = make_term(whole_cotangent, act_half).astype(jnp.bfloat16)
+    return sum_by_axis(term, SP).astype(jnp.float32)
 
 
 def on_device(features, weight_value, weight_gate, weight_out, conv_taps, norm_gain, out_grad):
@@ -118,19 +119,16 @@
         begin = 2 * half_width - offset
         mixed_grad = mixed_grad + conv_taps[offset] * grad_ext[begin : begin + row_count]
         taps_rows.append(jnp.sum(conv_grad * extended[offset : offset + row_count], axis=0))
-    taps_grad, gain_grad = (
-        total_of_pieces(jnp.stack(taps_rows), SP),
-        total_of_pieces(gain_part, SP),
-    )
+    small = lax.psum(jnp.concatenate([jnp.stack(taps_rows), gain_part[None]], axis=0), SP)
+    taps_grad, gain_grad = small[:tap_count], small[tap_count]
     value_grad = mixed_grad * gate_sig
     gate_grad = mixed_grad * value_pre * gate_sig * (1.0 - gate_sig)
     value_low = value_grad.astype(jnp.bfloat16)
     gate_low = gate_grad.astype(jnp.bfloat16)
     out_wgrad = out_weight_sum(whole_cotangent, act_half)
     both_low = jnp.concatenate([value_low, gate_low], axis=1)
-    joined = lax.psum_scatter(
-        make_term(whole_inputs, both_low), SP, scatter_dimension=0, tiled=True
-    )
+    joined = sum_by_axis(make_term(whole_inputs, both_low).astype(jnp.bfloat16), SP)
+    joined = joined.astype(jnp.float32)
     split_at = value_low.shape[1]
     value_wgrad = joined[:, :split_at]
     gate_wgrad = joined[:, split_at:]

time: 680 us -> 448 us (0.66)
  blocking collectives: 184 us -> 7.42 us
  waiting for transfers between devices: 402 us -> 347 us
    reduce_scatter x1 -> x0, waiting for transfers between devices: 267 us -> none  [on_device(): lax.psum_scatter(make_term(whole_inputs, both_low), SP, scatter_dimension...]
    all_gather x1 -> x0, blocking collectives: 177 us -> none  [total_of_pieces(): return lax.all_gather(x, axis).sum(0)]
    psum x0 -> x1, waiting for transfers between devices: none -> 128 us  [on_device(): lax.psum(jnp.concatenate([jnp.stack(taps_rows), gain_part[None]], axis=0)...]
    reduce_scatter x3 -> x6, waiting for transfers between devices: 104 us -> 188 us  [sum_by_axis(): running = lax.psum_scatter(running, axis, scatter_dimension=0, tiled=True)]
  transfers between devices with their start and end apart: 10 -> 12, of which waited for: 7 -> 11; matrix products, arithmetic and copies ran while one was open for 6% -> 8% of each run, Pallas kernels for 0% -> 0%
where the time goes in v1:
time: 448 us; the launch traced here: 447 us
  waiting for transfers between devices  347 us (77%)
  matrix products  32.2 us (7%)
  other arithmetic  26.2 us (6%)
  between operations  14.3 us (3%)
  starting transfers between devices  10.9 us (2%)
  local copies, waits for them, and re-layouts  8.86 us (2%)
  blocking collectives  7.42 us (2%)
    reduce_scatter x6, waiting for transfers between devices, sum_by_axis(): running = lax.psum_scatter(running, axis, scatter_dimension=0, tiled=True)  188 us
    psum x1, waiting for transfers between devices, on_device(): lax.psum(jnp.concatenate([jnp.stack(taps_rows), gain_part[None]], axis=0)...  128 us
    all_gather x1, waiting for transfers between devices, in_one_piece(): lax.all_gather(both, axis, axis=dim, tiled=True)  24.3 us
    dot_general x2, matrix products, make_term(): lax.dot_general(left_rows, right_rows, (((0,), (0,)), ((), ())), preferre...  16.9 us
  transfers between devices with their start and end apart: 12, of which 11 were waited for; matrix products, arithmetic and copies ran while one was open for 8% of the time, Pallas kernels for 0%

profile of v1, /device:TPU:0, one launch (start us, length us, event | category | flops | bytes accessed | tf_op | source)
XLA Modules:
  0.0 446.9 jit_solution(9746865256533950565)
XLA Ops:
  7.2 0.0 all-gather.2.cloned.1.call-start
  7.2 4.8 %pad_maximum_fusion = bf16[1024,2048]{1,0:T(8,128)(2,1)} fusion(bf16[512,2048]{1,0:T(8,128)(2,1)} %param.13, bf16[512,2048]{1,0:T(8,128)(2,1)} %param.7), kind=kLoop, calls=%fused_computation.30 | loop fusion | flops 8388608 | bytes 8388608 | tf_op jit(solution)/shard_map/concatenate | solution.py:24
  12.0 0.0 copy-start.1
  12.0 0.0 all-gather.2.cloned.1.call-update
  12.0 0.0 reduce-scatter.13.cloned.1.call-start
  12.1 0.8 copy-done.1
  12.9 24.3 %all-gather.2.cloned.1.call-done = bf16[1024,4096]{1,0:T(8,128)(2,1)} async-done(((bf16[1024,2048]{1,0:T(8,128)(2,1)}), bf16[1024,4096]{1,0:T(8,128)(2,1)}) %all-gather.2.cloned.1.call-update) | async-done | bytes 8388624 | tf_op jit(solution)/shard_map/all_gather | solution.py:25
  37.2 0.0 copy-start.3
  37.2 0.0 copy-start.4
  37.2 5.9 %fusion.14 = bf16[512,512]{1,0:T(8,128)(2,1)S(1)} fusion(bf16[4096,512]{1,0:T(8,128)(2,1)} %param.8, bf16[1024,4096]{1,0:T(8,128)(2,1)} %all-gather.2.cloned.1.call-done), kind=kOutput, calls=%fused_computation.43 | convolution fusion | flops 2147745792 | bytes 8912896 | tf_op jit(solution)/shard_map/dot_general | solution.py:76
  43.1 0.0 copy-done.3
  43.1 1.1 copy-done.4
  44.2 2.3 fusion.17
  46.6 0.3 fusion.20
  46.9 3.5 collective-permute-start
  50.4 1.3 collective-permute-start.1
  51.7 0.1 collective-permute-done
  51.8 4.2 collective-permute-done.1
  56.0 0.2 maximum_convert_fusion
  56.2 0.0 copy-start.2
  56.2 5.1 %fusion.121 = (f32[512]{0:T(512)S(1)}, f32[512]{0:T(512)S(1)}, f32[512,512]{1,0:T(8,128)S(1)}) fusion(f32[542,512]{1,0:T(8,128)S(1)} %maximum_convert_fusion, f32[512]{0:T(512)S(1)} %bitcast.127, f32[512]{0:T(512)S(1)} %bitcast.129, f32[512]{0:T(512)S(1)} %bitcast.71, f32[512]{0:T(512)S(1)} %bitcast.73, f32[512]{0:T(512)S(1)} %bitcast.75, ...), kind=kLoop, calls=%fused_computation.219 | loop fusion | flops 16776192 | bytes 33622016 | tf_op jit(solution)/shard_map/reduce_sum | solution.py:96
  61.2 0.0 copy-start
  61.3 3.7 all_to_all.12
  65.0 0.0 copy-done.2
  65.0 6.7 %convolution_convert_fusion.1 = bf16[4096,512]{1,0:T(8,128)(2,1)} fusion(bf16[1024,4096]{1,0:T(8,128)(2,1)} %all-gather.2.cloned.1.call-done, f32[512,512]{1,0:T(8,128)S(1)} %get-tuple-element.53, f32[512]{0:T(512)S(1)} %copy-done.2, f32[512]{0:T(512)S(1)} %get-tuple-element.94, f32[512]{0:T(512)S(1)} %get-tuple-element.93), kind=kOutput, calls=%fused_computation.29 | convolution fusion | flops 2151677952 | bytes 9443328 | tf_op jit(solution)/shard_map/dot_general | solution.py:64
  71.7 0.0 reduce-scatter.13.cloned.1.call-update
  71.8 0.0 reduce-scatter.7.cloned.1.call-start
  71.8 0.0 copy-done
  71.8 7.1 %multiply_reduce_fusion = (f32[512]{0:T(512)S(1)}, f32[512]{0:T(512)S(1)}, f32[512]{0:T(512)S(1)}, f32[512,512]{1,0:T(8,128)}) fusion(f32[512,512]{1,0:T(8,128)S(1)} %get-tuple-element.53, f32[512]{0:T(512)S(1)} %get-tuple-element.94, f32[512]{0:T(512)S(1)} %get-tuple-element.93, f32[512]{0:T(512)S(1)} %copy-done.2, bf16[4096,512]{1,0:T(8,128)(2,1)} %param.10, ...), kind=kOutput, calls=%fused_computation.164 | convolution fusion | flops 2151938560 | bytes 10498048 | tf_op jit(solution)/shard_map/dot_general | solution.py:105
  79.0 3.7 all_to_all.13
  82.7 4.2 multiply_reduce_fusion.1
  86.9 1.3 collective-permute-start.2
  88.2 4.5 %collective-permute-start.3 = (f32[15,512]{1,0:T(8,128)S(1)}, f32[15,512]{1,0:T(8,128)S(1)}, u32[]{:S(2)}, u32[]{:S(2)}) collective-permute-start(f32[15,512]{1,0:T(8,128)S(1)} %get-tuple-element.55), channel_id=1, source_target_pairs={{0,2},{2,4},{4,6},{6,8},{8,10},{10,12},{12,14},{14,16},{16,18},{18... | collective-permute-start | bytes 92168 | tf_op jit(solution)/shard_map/ppermute | solution.py:33
  92.8 0.0 collective-permute-done.2
  92.8 1.6 collective-permute-done.3
  94.4 5.9 %fusion.122 = (bf16[512,512]{1,0:T(8,128)(2,1)}, f32[512,512]{1,0:T(8,128)}, f32[512,512]{1,0:T(8,128)}) fusion(bf16[512,512]{1,0:T(8,128)(2,1)S(1)} %fusion.17, f32[512,512]{1,0:T(8,128)S(1)} %get-tuple-element.47, f32[15,512]{1,0:T(8,128)S(1)} %collective-permute-done.3, f32[512]{0:T(512)S(1)} %bitcast.128, f32[512]{0:T(512)S(1)} %bitcast.130, ...), kind=kLoop, calls=%fused_computation.220 | loop fusion | flops 25427968 | bytes 4319232 | tf_op jit(solution)/shard_map/convert_element_type | solution.py:126
  100.2 2.6 fusion.125
  102.8 10.2 %convolution_convert_fusion = bf16[4096,1024]{1,0:T(8,128)(2,1)} fusion(bf16[1024,4096]{1,0:T(8,128)(2,1)} %all-gather.2.cloned.1.call-done, bf16[512,512]{1,0:T(8,128)(2,1)S(1)} %get-tuple-element.51, bf16[512,512]{1,0:T(8,128)(2,1)} %get-tuple-element.48), kind=kOutput, calls=%fused_computation | convolution fusion | flops 4301258752 | bytes 13631488 | tf_op jit(solution)/shard_map/dot_general | solution.py:64
  113.0 0.0 reduce-scatter.7.cloned.1.call-update
  113.0 0.0 reduce-scatter.15.cloned.1.call-start
  113.0 10.5 %reduce-scatter.13.cloned.1.call-done = bf16[1024,512]{1,0:T(8,128)(2,1)} async-done(((bf16[4096,512]{1,0:T(8,128)(2,1)}), bf16[1024,512]{1,0:T(8,128)(2,1)}) %reduce-scatter.13.cloned.1.call-update) | async-done | bytes 1048592 | tf_op jit(solution)/shard_map/reduce_scatter | solution.py:15
  123.6 0.0 reduce-scatter.15.cloned.1.call-update
  123.6 0.0 reduce-scatter.9.cloned.1.call-start
  123.7 82.9 %reduce-scatter.7.cloned.1.call-done = bf16[1024,1024]{1,0:T(8,128)(2,1)} async-done(((bf16[4096,1024]{1,0:T(8,128)(2,1)}), bf16[1024,1024]{1,0:T(8,128)(2,1)}) %reduce-scatter.7.cloned.1.call-update) | async-done | bytes 2097168 | tf_op jit(solution)/shard_map/reduce_scatter | solution.py:15
  206.6 0.0 reduce-scatter.9.cloned.1.call-update
  206.6 0.0 all-reduce.2.cloned.1.call-start
  206.7 1.7 multiply_reduce_fusion.2
  208.4 2.5 concatenate.60
  210.9 0.0 all-reduce.2.cloned.1.call-update
  210.9 0.0 reduce-scatter.17.cloned.1.call-start
  211.0 21.2 %reduce-scatter.15.cloned.1.call-done = bf16[256,512]{1,0:T(8,128)(2,1)} async-done(((bf16[1024,512]{1,0:T(8,128)(2,1)}), bf16[256,512]{1,0:T(8,128)(2,1)}) %reduce-scatter.15.cloned.1.call-update) | async-done | bytes 262160 | tf_op jit(solution)/shard_map/reduce_scatter | solution.py:15
  232.2 0.0 reduce-scatter.17.cloned.1.call-update
  232.2 0.0 reduce-scatter.11.cloned.1.call-start
  232.3 31.7 %reduce-scatter.9.cloned.1.call-done = bf16[256,1024]{1,0:T(8,128)(2,1)} async-done(((bf16[1024,1024]{1,0:T(8,128)(2,1)}), bf16[256,1024]{1,0:T(8,128)(2,1)}) %reduce-scatter.9.cloned.1.call-update) | async-done | bytes 524304 | tf_op jit(solution)/shard_map/reduce_scatter | solution.py:15
  264.0 0.0 reduce-scatter.11.cloned.1.call-update
  264.0 128.1 %all-reduce.2.cloned.1.call-done = f32[32,512]{1,0:T(8,128)} async-done(((f32[32,512]{1,0:T(8,128)}), f32[32,512]{1,0:T(8,128)}) %all-reduce.2.cloned.1.call-update) | async-done | bytes 65552 | tf_op jit(solution)/shard_map/psum | solution.py:122
  392.1 1.3 slice.602
  393.4 19.8 %reduce-scatter.17.cloned.1.call-done = bf16[64,512]{1,0:T(8,128)(2,1)} async-done(((bf16[256,512]{1,0:T(8,128)(2,1)}), bf16[64,512]{1,0:T(8,128)(2,1)}) %reduce-scatter.17.cloned.1.call-update) | async-done | bytes 65552 | tf_op jit(solution)/shard_map/reduce_scatter | solution.py:15
  413.2 1.5 convert_element_type.51
  414.7 22.3 %reduce-scatter.11.cloned.1.call-done = bf16[64,1024]{1,0:T(8,128)(2,1)} async-done(((bf16[256,1024]{1,0:T(8,128)(2,1)}), bf16[64,1024]{1,0:T(8,128)(2,1)}) %reduce-scatter.11.cloned.1.call-update) | async-done | bytes 131088 | tf_op jit(solution)/shard_map/reduce_scatter | solution.py:15
  437.0 1.6 fusion.129
  438.6 1.5 copy.23
  (12 shorter events, 0.1 us)
Async XLA Ops:
  7.2 30.0 %all-gather.2.cloned.1.call-start = ((), (), s32[]{:S(2)}) async-start(), calls=%async_computation.8 | async-start | bytes 12582912 | tf_op jit(solution)/shard_map/all_gather | solution.py:25
  12.0 0.8 copy-start.1
  12.0 111.6 %reduce-scatter.13.cloned.1.call-start = ((), (), s32[]{:S(2)}) async-start(), calls=%async_computation.12 | async-start | bytes 5242880 | tf_op jit(solution)/shard_map/reduce_scatter | solution.py:15
  37.2 5.9 %copy-start.3 = (bf16[1024,4096]{1,0:T(8,128)(2,1)S(1)}, bf16[1024,4096]{1,0:T(8,128)(2,1)}, u32[]{:S(2)}) copy-start(bf16[1024,4096]{1,0:T(8,128)(2,1)} %all-gather.2.cloned.1.call-done) | copy-start | bytes 25165828
  37.2 7.0 %copy-start.4 = (bf16[4096,512]{1,0:T(8,128)(2,1)S(1)}, bf16[4096,512]{1,0:T(8,128)(2,1)}, u32[]{:S(2)}) copy-start(bf16[4096,512]{1,0:T(8,128)(2,1)} %param.9) | copy-start | bytes 12582916
  46.9 4.9 %collective-permute-start = (bf16[15,512]{1,0:T(8,128)(2,1)S(1)}, bf16[15,512]{1,0:T(8,128)(2,1)S(1)}, u32[]{:S(2)}, u32[]{:S(2)}) collective-permute-start(bf16[15,512]{1,0:T(8,128)(2,1)S(1)} %get-tuple-element.56), channel_id=1, source_target_pairs={{0,2},{2,4},{4,6},{6,8},{8,10},{10,12},{12,14},{14,16},{16,18},{18... | collective-permute-start | bytes 46088 | tf_op jit(solution)/shard_map/ppermute | solution.py:33
  50.4 5.6 %collective-permute-start.1 = (bf16[15,512]{1,0:T(8,128)(2,1)S(1)}, bf16[15,512]{1,0:T(8,128)(2,1)S(1)}, u32[]{:S(2)}, u32[]{:S(2)}) collective-permute-start(bf16[15,512]{1,0:T(8,128)(2,1)S(1)} %get-tuple-element.57), channel_id=1, source_target_pairs={{2,0},{4,2},{6,4},{8,6},{10,8},{12,10},{14,12},{16,14},{18,16},{20... | collective-permute-start | bytes 46088 | tf_op jit(solution)/shard_map/ppermute | solution.py:36
  56.2 8.9 %copy-start.2 = (f32[512]{0:T(512)S(1)}, f32[512]{0:T(512)}, u32[]{:S(2)}) copy-start(f32[512]{0:T(512)} %param.12) | copy-start | bytes 6148
  61.2 10.6 %copy-start = (f32[512,512]{1,0:T(8,128)}, f32[512,512]{1,0:T(8,128)S(1)}, u32[]{:S(2)}) copy-start(f32[512,512]{1,0:T(8,128)S(1)} %get-tuple-element.53) | copy-start | bytes 3145732
  71.8 134.8 %reduce-scatter.7.cloned.1.call-start = ((), (), s32[]{:S(2)}) async-start(), calls=%async_computation.9 | async-start | bytes 10485760 | tf_op jit(solution)/shard_map/reduce_scatter | solution.py:15
  86.9 5.9 %collective-permute-start.2 = (f32[15,512]{1,0:T(8,128)S(1)}, f32[15,512]{1,0:T(8,128)S(1)}, u32[]{:S(2)}, u32[]{:S(2)}) collective-permute-start(f32[15,512]{1,0:T(8,128)S(1)} %get-tuple-element.54), channel_id=1, source_target_pairs={{2,0},{4,2},{6,4},{8,6},{10,8},{12,10},{14,12},{16,14},{18,16},{20... | collective-permute-start | bytes 92168 | tf_op jit(solution)/shard_map/ppermute | solution.py:36
  88.2 6.1 %collective-permute-start.3 = (f32[15,512]{1,0:T(8,128)S(1)}, f32[15,512]{1,0:T(8,128)S(1)}, u32[]{:S(2)}, u32[]{:S(2)}) collective-permute-start(f32[15,512]{1,0:T(8,128)S(1)} %get-tuple-element.55), channel_id=1, source_target_pairs={{0,2},{2,4},{4,6},{6,8},{8,10},{10,12},{12,14},{14,16},{16,18},{18... | collective-permute-start | bytes 92168 | tf_op jit(solution)/shard_map/ppermute | solution.py:33
  113.0 119.2 %reduce-scatter.15.cloned.1.call-start = ((), (), s32[]{:S(2)}) async-start(), calls=%async_computation.13 | async-start | bytes 1310720 | tf_op jit(solution)/shard_map/reduce_scatter | solution.py:15
  123.6 140.4 %reduce-scatter.9.cloned.1.call-start = ((), (), s32[]{:S(2)}) async-start(), calls=%async_computation.10 | async-start | bytes 2621440 | tf_op jit(solution)/shard_map/reduce_scatter | solution.py:15
  206.6 185.5 %all-reduce.2.cloned.1.call-start = ((), (), s32[]{:S(2)}) async-start(), calls=%async_computation.15 | async-start | bytes 131072 | tf_op jit(solution)/shard_map/psum | solution.py:122
  210.9 202.3 %reduce-scatter.17.cloned.1.call-start = ((), (), s32[]{:S(2)}) async-start(), calls=%async_computation.14 | async-start | bytes 327680 | tf_op jit(solution)/shard_map/reduce_scatter | solution.py:15
  232.2 204.7 %reduce-scatter.11.cloned.1.call-start = ((), (), s32[]{:S(2)}) async-start(), calls=%async_computation.11 | async-start | bytes 655360 | tf_op jit(solution)/shard_map/reduce_scatter | solution.py:15
Sparse Core Ops, SparseCore 0:
  12.1 25.0 all-gather.1
  71.9 51.6 reduce-scatter.12
  126.1 80.4 reduce-scatter.6
  208.8 23.3 reduce-scatter.14
  234.5 29.4 reduce-scatter.8
  269.1 123.0 all-reduce.1
  394.5 18.6 reduce-scatter.16
  415.6 21.3 reduce-scatter.10

commit v2 on v1

--- a/solution.py
+++ b/solution.py
@@ -1,19 +1,301 @@
+import functools
+
 import jax
 import jax.numpy as jnp
 from jax import lax
-from jax.sharding import Mesh
+from jax.experimental import pallas as pl
+from jax.experimental.pallas import tpu as pltpu
 from jax.sharding import PartitionSpec as P
 
-SP = ("sp_0", "sp_1", "sp_2")
-
+SP = "sp"
+MESH = pl.DeviceIdType.MESH
+BF16 = jnp.bfloat16
+F32 = jnp.float32
 
 NORM_EPS = 1e-05
 
-
-def sum_by_axis(running, axes):
-    for axis in axes:
-        running = lax.psum_scatter(running, axis, scatter_dimension=0, tiled=True)
-    return running
+WIDTHS = ((128, 128, 256), (256, 128, 128), (128, 256, 128))
+ORDERS = ("xzy", "yxz", "zyx")
+ROWS = (512, 128, 32)
+SENT = (BF16, BF16, F32)
+
+
+def coords():
+    sp = lax.axis_index("sp")
+    return {"z": sp // 16, "y": (sp // 4) % 4, "x": sp % 4}
+
+
+def peer(where, dim, shift):
+    to = dict(where)
+    to[dim] = (where[dim] + shift + 4) % 4
+    return (to["z"] * 16 + to["y"] * 4 + to["x"], lax.axis_index("tp"))
+
+
+def remote(src, dst, ssem, rsem, device):
+    return pltpu.make_async_remote_copy(
+        src_ref=src, dst_ref=dst, send_sem=ssem, recv_sem=rsem,
+        device_id=device, device_id_type=MESH,
+    )
+
+
+class Part:
+    def __init__(self, where, p, lhs_t, rhs, cols, out, bufs, sems):
+        self.where, self.p, self.lhs_t, self.rhs = where, p, lhs_t, rhs
+        self.cols, self.out, self.bufs, self.sems = cols, out, bufs, sems
+
+    def source(self, stage, h, j):
+        off, width = self.cols
+        if stage == 0:
+            if self.p == 0:
+                rows = self.lhs_t[pl.ds(2 * h, 2), :, j]
+            elif self.p == 1:
+                rows = self.lhs_t[:, j, pl.ds(2 * h, 2)]
+            else:
+                rows = self.lhs_t[j, pl.ds(2 * h, 2)]
+            rows = rows.reshape(512, rows.shape[-1])
+            return jnp.dot(rows, self.rhs[:, off : off + width], preferred_element_type=F32)
+        held = self.bufs[stage - 1][2]
+        if stage == 1:
+            if self.p == 1:
+                at = (j // 2) * 8 + j % 2
+                two = [held[at + 2 * (2 * h + i)] for i in range(2)]
+                return jnp.concatenate(two, axis=0)
+            return held[pl.ds(4 * j + 2 * h, 2)].reshape(128, width)
+        return held[j, pl.ds(pl.multiple_of(h * 32, 32), 32)]
+
+    def place(self, stage, h, value):
+        off, width = self.cols
+        if stage == 2:
+            self.out[pl.ds(pl.multiple_of(h * 32, 32), 32), off : off + width] = value
+            return
+        held = self.bufs[stage][2]
+        count = ROWS[stage] // 64
+        held[pl.ds(count * h, count)] = value.reshape(count, 64, width)
+
+    def copy(self, stage, slot, sign):
+        send, recv, _ = self.bufs[stage]
+        ssem, rsem = self.sems
+        at = stage * 6 + slot
+        dim = ORDERS[self.p][stage]
+        return remote(
+            send.at[slot], recv.at[slot], ssem.at[at], rsem.at[at],
+            peer(self.where, dim, sign),
+        )
+
+    def first(self, stage):
+        m = self.where[ORDERS[self.p][stage]]
+        send = self.bufs[stage][0]
+
+        @pl.loop(0, 4)
+        def _(i):
+            sign = 1 - 2 * (i % 2)
+            h = ((i + 1) // 2) % 2
+            j = (m + 6 - (i // 2) * sign) % 4
+            send[i] = self.source(stage, h, j).astype(SENT[stage])
+            self.copy(stage, i, sign).start()
+
+    def second(self, stage):
+        m = self.where[ORDERS[self.p][stage]]
+        send, recv, _ = self.bufs[stage]
+
+        @pl.loop(0, 2)
+        def _(k):
+            sign = 1 - 2 * k
+            self.copy(stage, k, sign).wait_recv()
+            mine = self.source(stage, k, (m + 4 + sign) % 4)
+            send[4 + k] = (mine + recv[k].astype(F32)).astype(SENT[stage])
+            self.copy(stage, 4 + k, sign).start()
+
+    def third(self, stage):
+        m = self.where[ORDERS[self.p][stage]]
+        recv = self.bufs[stage][1]
+
+        @pl.loop(0, 2)
+        def _(h):
+            mine = self.source(stage, h, m)
+            self.copy(stage, 3 - h, 1).wait_recv()
+            self.copy(stage, 4 + h, 1).wait_recv()
+            total = mine + recv[3 - h].astype(F32) + recv[4 + h].astype(F32)
+            self.place(stage, h, total)
+
+    def drain(self):
+        for stage in range(3):
+            @pl.loop(0, 6)
+            def _(slot):
+                self.copy(stage, slot, 1).wait_send()
+
+
+class Small:
+    def __init__(self, where, start, cols, slots, sums, out, sems):
+        self.where, self.start, self.cols, self.slots = where, start, cols, slots
+        self.sums, self.out, self.sems = sums, out, sems
+
+    def copy(self, stage, d):
+        dim = "xyzx"[stage]
+        mine = self.where[dim]
+        ssem, rsem = self.sems
+        src = self.cols.at[(mine + d) % 4] if stage == 0 else self.sums.at[stage - 1]
+        at = stage * 4 + d
+        return remote(src, self.slots.at[stage, mine], ssem.at[at], rsem.at[at],
+                      peer(self.where, dim, d))
+
+    def send(self, stage):
+        mine = self.where["xyzx"[stage]]
+        if stage == 0:
+            for j in range(4):
+                self.cols[j] = self.start[:, 128 * j : 128 * j + 128]
+            self.slots[0, mine] = self.cols[mine]
+        else:
+            self.slots[stage, mine] = self.sums[stage - 1]
+
+        @pl.loop(1, 4)
+        def _(d):
+            self.copy(stage, d).start()
+
+    def collect(self, stage):
+        @pl.loop(1, 4)
+        def _(d):
+            self.copy(stage, d).wait_recv()
+
+        if stage < 3:
+            a, b, c, d = [self.slots[stage, j] for j in range(4)]
+            self.sums[stage] = (a + b) + (c + d)
+        else:
+            for j in range(4):
+                self.out[:, 128 * j : 128 * j + 128] = self.slots[3, j]
+
+    def drain(self):
+        for stage in range(4):
+            @pl.loop(1, 4)
+            def _(d):
+                self.copy(stage, d).wait_send()
+
+
+def transpose_into(src, dst):
+    @pl.loop(0, 16)
+    def _(i):
+        cols = src[:, pl.ds(pl.multiple_of(i * 256, 256), 256)]
+        dst[i // 4, i % 4] = cols.T.reshape(4, 64, src.shape[0])
+
+
+def greet(where):
+    barrier = pltpu.get_barrier_semaphore()
+    for dim in "zyx":
+        for shift in (1, 2, 3):
+            pl.semaphore_signal(
+                barrier, inc=1, device_id=peer(where, dim, shift), device_id_type=MESH
+            )
+    pl.semaphore_wait(barrier, 9)
+
+
+def part_scratch():
+    shapes = []
+    for widths in WIDTHS:
+        for width in widths:
+            for stage in range(3):
+                shapes.append(pltpu.VMEM((6, ROWS[stage], width), SENT[stage]))
+                shapes.append(pltpu.VMEM((6, ROWS[stage], width), SENT[stage]))
+                if stage < 2:
+                    shapes.append(pltpu.VMEM((ROWS[stage] // 32, 64, width), F32))
+            shapes.append(pltpu.SemaphoreType.DMA((18,)))
+            shapes.append(pltpu.SemaphoreType.DMA((18,)))
+    return shapes
+
+
+def take_parts(where, r, lhs_t, rhs, out, pool):
+    parts, off = [], 0
+    for p, width in enumerate(WIDTHS[r]):
+        bufs = []
+        for stage in range(3):
+            send, recv = next(pool), next(pool)
+            bufs.append((send, recv, next(pool) if stage < 2 else None))
+        sems = (next(pool), next(pool))
+        parts.append(Part(where, p, lhs_t, rhs, (off, width), out, bufs, sems))
+        off += width
+    return parts
+
+
+def wgrad_kernel(feat, cot, act, value_low, gate_low, small,
+                 value_out, gate_out, out_out, small_out, feat_t, cot_t,
+                 cols, slots, sums, small_ssem, small_rsem, *pool):
+    where = coords()
+    greet(where)
+    pool = iter(pool)
+    tiny = Small(where, small, cols, slots, sums, small_out, (small_ssem, small_rsem))
+    tiny.send(0)
+    transpose_into(cot, cot_t)
+    rounds = [
+        take_parts(where, 0, cot_t, act, out_out, pool),
+        take_parts(where, 1, feat_t, value_low, value_out, pool),
+        take_parts(where, 2, feat_t, gate_low, gate_out, pool),
+    ]
+
+    def run(name, r, stage):
+        for part in rounds[r]:
+            getattr(part, name)(stage)
+
+    run("first", 0, 0)
+    transpose_into(feat, feat_t)
+    run("first", 1, 0)
+    run("second", 0, 0)
+    run("first", 2, 0)
+    run("second", 1, 0)
+    run("second", 2, 0)
+    tiny.collect(0)
+    tiny.send(1)
+    run("third", 0, 0)
+    run("first", 0, 1)
+    tiny.collect(1)
+    tiny.send(2)
+    run("third", 1, 0)
+    run("first", 1, 1)
+    run("second", 0, 1)
+    run("third", 2, 0)
+    run("first", 2, 1)
+    tiny.collect(2)
+    tiny.send(3)
+    run("third", 0, 1)
+    run("first", 0, 2)
+    run("second", 1, 1)
+    run("second", 2, 1)
+    run("third", 1, 1)
+    run("first", 1, 2)
+    run("second", 0, 2)
+    run("third", 2, 1)
+    run("first", 2, 2)
+    run("second", 1, 2)
+    run("second", 2, 2)
+    tiny.collect(3)
+    for r in range(3):
+        run("third", r, 2)
+    tiny.drain()
+    for parts in rounds:
+        for part in parts:
+            part.drain()
+
+
+def weight_grads(feat, cot, act, value_low, gate_low, small):
+    shape = jax.ShapeDtypeStruct((64, 512), F32)
+    vmem = pl.BlockSpec(memory_space=pltpu.VMEM)
+    return pl.pallas_call(
+        wgrad_kernel,
+        out_shape=(shape, shape, shape, jax.ShapeDtypeStruct((32, 512), F32)),
+        in_specs=[vmem] * 6,
+        out_specs=(vmem,) * 4,
+        scratch_shapes=[
+            pltpu.VMEM((4, 4, 4, 64, 512), BF16),
+            pltpu.VMEM((4, 4, 4, 64, 512), BF16),
+            pltpu.VMEM((4, 32, 128), F32),
+            pltpu.VMEM((4, 4, 32, 128), F32),
+            pltpu.VMEM((3, 32, 128), F32),
+            pltpu.SemaphoreType.DMA((16,)),
+            pltpu.SemaphoreType.DMA((16,)),
+            *part_scratch(),
+        ],
+        compiler_params=pltpu.CompilerParams(
+            collective_id=0, has_side_effects=True, vmem_limit_bytes=64 * 1024 * 1024 - 65536
+        ),
+    )(feat, cot, act, value_low, gate_low, small)
 
 
 def in_one_piece(arrays, axis, dim, along):
@@ -56,21 +338,6 @@
     return tuple(finished)
 
 
-def total_of_pieces(x, axis):
-    return lax.all_gather(x, axis).sum(0)
-
-
-def make_term(left_rows, right_rows):
-    return lax.dot_general(
-        left_rows, right_rows, (((0,), (0,)), ((), ())), preferred_element_type=jnp.float32
-    )
-
-
-def out_weight_sum(whole_cotangent, act_half):
-    term = make_term(whole_cotangent, act_half).astype(jnp.bfloat16)
-    return sum_by_axis(term, SP).astype(jnp.float32)
-
-
 def on_device(features, weight_value, weight_gate, weight_out, conv_taps, norm_gain, out_grad):
     whole_inputs, whole_cotangent = in_one_piece((features, out_grad), "tp", 1, 0)
     value_half = jnp.dot(whole_inputs, weight_value, preferred_element_type=jnp.float32).astype(
@@ -88,7 +355,7 @@
     half_width = tap_count // 2
     row_count = mixed_half.shape[0]
     channels = mixed_half.shape[1] * lax.axis_size("tp")
-    extended = with_halo(mixed_half, ((SP, 0),), half_width).astype(jnp.float32)
+    extended = with_halo(mixed_half, (("sp", 0),), half_width).astype(jnp.float32)
     conv_out = jnp.zeros(mixed_half.shape, jnp.float32)
     for offset in range(tap_count):
         conv_out = conv_out + conv_taps[offset] * extended[offset : offset + row_count]
@@ -112,34 +379,29 @@
     first_mom = first_sum[:, None] / channels
     second_mom = second_sum[:, None] / channels
     conv_grad = inv_std * (norm_grad - first_mom - normed * second_mom)
-    grad_ext = with_halo(conv_grad, ((SP, 0),), half_width)
+    grad_ext = with_halo(conv_grad, (("sp", 0),), half_width)
     mixed_grad = jnp.zeros(conv_grad.shape, jnp.float32)
     taps_rows = []
     for offset in range(tap_count):
         begin = 2 * half_width - offset
         mixed_grad = mixed_grad + conv_taps[offset] * grad_ext[begin : begin + row_count]
         taps_rows.append(jnp.sum(conv_grad * extended[offset : offset + row_count], axis=0))
-    small = lax.psum(jnp.concatenate([jnp.stack(taps_rows), gain_part[None]], axis=0), SP)
-    taps_grad, gain_grad = small[:tap_count], small[tap_count]
     value_grad = mixed_grad * gate_sig
     gate_grad = mixed_grad * value_pre * gate_sig * (1.0 - gate_sig)
     value_low = value_grad.astype(jnp.bfloat16)
     gate_low = gate_grad.astype(jnp.bfloat16)
-    out_wgrad = out_weight_sum(whole_cotangent, act_half)
-    both_low = jnp.concatenate([value_low, gate_low], axis=1)
-    joined = sum_by_axis(make_term(whole_inputs, both_low).astype(jnp.bfloat16), SP)
-    joined = joined.astype(jnp.float32)
-    split_at = value_low.shape[1]
-    value_wgrad = joined[:, :split_at]
-    gate_wgrad = joined[:, split_at:]
+    small = jnp.concatenate([jnp.stack(taps_rows), gain_part[None]], axis=0)
+    value_wgrad, gate_wgrad, out_wgrad, small = weight_grads(
+        whole_inputs, whole_cotangent, act_half, value_low, gate_low, small
+    )
+    taps_grad, gain_grad = small[:tap_count], small[tap_count]
     return (value_grad, gate_grad, value_wgrad, gate_wgrad, out_wgrad, taps_grad, gain_grad)
 
 
 def solution(mesh):
-    split = Mesh(mesh.devices.reshape(4, 4, 4, mesh.shape["tp"]), ("sp_0", "sp_1", "sp_2", "tp"))
     return jax.shard_map(
         on_device,
-        mesh=split,
+        mesh=mesh,
         in_specs=(
             P(SP, "tp"),
             P(None, "tp"),

time: 448 us -> 200 us (0.45)
  waiting for transfers between devices: 347 us -> 24.9 us
  Pallas kernels: 0 us -> 84.3 us
  matrix products: 32.2 us -> 16.2 us
  local copies, waits for them, and re-layouts: 8.86 us -> 17.8 us
    reduce_scatter x6 -> x0, waiting for transfers between devices: 188 us -> none  [sum_by_axis(): running = lax.psum_scatter(running, axis, scatter_dimension=0, tiled=True)]
    psum x1 -> x0, waiting for transfers between devices: 128 us -> none  [on_device(): lax.psum(jnp.concatenate([jnp.stack(taps_rows), gain_part[None]], axis=0)...]
    pallas_call x0 -> x1, Pallas kernels: none -> 84.3 us  [weight_grads(): pl.pallas_call(wgrad_kernel, out_shape=(shape, shape, shape, jax.ShapeDty...]
    dot_general x2 -> x0, matrix products: 16.9 us -> none  [make_term(): lax.dot_general(left_rows, right_rows, (((0,), (0,)), ((), ())), preferre...]
    unnamed x11 -> x14, local copies, waits for them, and re-layouts: 3.34 us -> 8.09 us
  transfers between devices with their start and end apart: 12 -> 5, of which waited for: 11 -> 2; matrix products, arithmetic and copies ran while one was open for 8% -> 5% of each run, Pallas kernels for 0% -> 0%
where the time goes in v2:
time: 200 us
  Pallas kernels  84.3 us (42%)
  waiting for transfers between devices  24.9 us (12%)
  other arithmetic  24.1 us (12%)
  local copies, waits for them, and re-layouts  17.8 us (9%)
  matrix products  16.2 us (8%)
  between operations  14.2 us (7%)
  starting transfers between devices  10.9 us (5%)
  blocking collectives  7.42 us (4%)
    pallas_call x1, Pallas kernels, weight_grads(): pl.pallas_call(wgrad_kernel, out_shape=(shape, shape, shape, jax.ShapeDty...  84.3 us
    all_gather x1, waiting for transfers between devices, in_one_piece(): lax.all_gather(both, axis, axis=dim, tiled=True)  24.3 us
    ppermute x2, starting transfers between devices, with_halo(): lax.ppermute(lax.slice_in_dim(block, block.shape[dim] - width, None, axis...  8.25 us
    unnamed x14, local copies, waits for them, and re-layouts  8.09 us
    dot_general x1, matrix products, on_device(): jnp.dot(whole_cotangent, weight_out, preferred_element_type=jnp.float32)  7.93 us
    all_to_all x2, blocking collectives, from_everyone(): lax.all_to_all(jnp.broadcast_to(x[None], (devices, *x.shape)), axis, 0, 0...  7.42 us
    reduce_sum x2, other arithmetic, on_device(): jnp.sum(conv_grad * extended[offset:offset + row_count], axis=0)  6.51 us
    dot_general x1, matrix products, on_device(): jnp.dot(whole_inputs, weight_gate, preferred_element_type=jnp.float32)  5.92 us
  transfers between devices with their start and end apart: 5, of which 2 were waited for; matrix products, arithmetic and copies ran while one was open for 5% of the time, Pallas kernels for 0%

profile of v2, /device:TPU:0, one launch (start us, length us, event | category | flops | bytes accessed | tf_op | source)
XLA Modules:
  0.0 199.9 jit_solution(16107006923846449864)
XLA Ops:
  7.2 0.0 all-gather.2.cloned.1.call-start
  7.2 4.8 %pad_maximum_fusion = bf16[1024,2048]{1,0:T(8,128)(2,1)} fusion(bf16[512,2048]{1,0:T(8,128)(2,1)} %param.13, bf16[512,2048]{1,0:T(8,128)(2,1)} %param.7), kind=kLoop, calls=%fused_computation.28 | loop fusion | flops 8388608 | bytes 8388608 | tf_op jit(solution)/shard_map/concatenate | solution.py:306
  12.0 0.0 copy-start.2
  12.0 0.0 all-gather.2.cloned.1.call-update
  12.0 0.8 copy-done.2
  12.9 24.3 %all-gather.2.cloned.1.call-done = bf16[1024,4096]{1,0:T(8,128)(2,1)} async-done(((bf16[1024,2048]{1,0:T(8,128)(2,1)}), bf16[1024,4096]{1,0:T(8,128)(2,1)}) %all-gather.2.cloned.1.call-update) | async-done | bytes 8388624 | tf_op jit(solution)/shard_map/all_gather | solution.py:307
  37.2 0.0 copy-start
  37.2 0.0 copy-start.4
  37.2 5.9 %convolution_convert_fusion = bf16[512,512]{1,0:T(8,128)(2,1)S(1)} fusion(bf16[4096,512]{1,0:T(8,128)(2,1)} %param.9, bf16[1024,4096]{1,0:T(8,128)(2,1)} %all-gather.2.cloned.1.call-done), kind=kOutput, calls=%fused_computation.33 | convolution fusion | flops 2147745792 | bytes 8912896 | tf_op jit(solution)/shard_map/dot_general | solution.py:346
  43.1 0.0 copy-done
  43.1 1.1 copy-done.4
  44.2 2.3 %convolution_convert_fusion.1 = bf16[512,512]{1,0:T(8,128)(2,1)S(1)} fusion(bf16[4096,512]{1,0:T(8,128)(2,1)S(1)} %copy-done.4, bf16[1024,4096]{1,0:T(8,128)(2,1)S(1)} %copy-done), kind=kOutput, calls=%fused_computation.34 | convolution fusion | flops 2147745792 | bytes 8912896 | tf_op jit(solution)/shard_map/dot_general | solution.py:343
  46.6 0.3 fusion.1
  46.9 3.5 %collective-permute-start = (bf16[15,512]{1,0:T(8,128)(2,1)S(1)}, bf16[15,512]{1,0:T(8,128)(2,1)S(1)}, u32[]{:S(2)}, u32[]{:S(2)}) collective-permute-start(bf16[15,512]{1,0:T(8,128)(2,1)S(1)} %get-tuple-element.67), channel_id=1, source_target_pairs={{0,2},{2,4},{4,6},{6,8},{8,10},{10,12},{12,14},{14,16},{16,18},{18... | collective-permute-start | bytes 46088 | tf_op jit(solution)/shard_map/ppermute | solution.py:315
  50.4 1.3 collective-permute-start.1
  51.7 3.7 %fusion.102 = (bf16[512,4096]{1,0:T(8,128)(2,1)}, bf16[512,4096]{1,0:T(8,128)(2,1)}) fusion(bf16[1024,4096]{1,0:T(8,128)(2,1)S(1)} %copy-done), kind=kLoop, calls=%fused_computation.206 | loop fusion | bytes 16777216 | tf_op jit(solution)/shard_map/split | solution.py:307
  55.4 0.0 collective-permute-done
  55.4 0.6 collective-permute-done.1
  56.0 0.2 maximum_convert_fusion
  56.2 0.0 copy-start.3
  56.2 5.1 %fusion.96 = (f32[512]{0:T(512)S(1)}, f32[512]{0:T(512)S(1)}, f32[512,512]{1,0:T(8,128)S(1)}) fusion(f32[542,512]{1,0:T(8,128)S(1)} %maximum_convert_fusion, f32[512]{0:T(512)S(1)} %bitcast.89, f32[512]{0:T(512)S(1)} %bitcast.91, f32[512]{0:T(512)S(1)} %bitcast.95, f32[512]{0:T(512)S(1)} %bitcast.97, f32[512]{0:T(512)S(1)} %bitcast.99, ...), kind=kLoop, calls=%fused_computation.203 | loop fusion | flops 16776192 | bytes 33622016 | tf_op jit(solution)/shard_map/reduce_sum | solution.py:363
  61.2 0.0 copy-start.1
  61.3 3.7 %all_to_all.12 = f32[2,1,1024]{2,1,0:T(1,128)S(1)} all-to-all(f32[2,1,1024]{2,1,0:T(1,128)S(1)} %broadcast_in_dim.6), channel_id=1, replica_groups=mesh['sp'=64,'tp'=2] {'tp'}, dimensions={0} | all-to-all | bytes 16384 | tf_op jit(solution)/shard_map/all_to_all | solution.py:325
  65.0 0.0 copy-done.3
  65.0 7.9 %multiply_reduce_fusion = (f32[512]{0:T(512)}, f32[512]{0:T(512)S(1)}, f32[512]{0:T(512)S(1)}, bf16[512,512]{1,0:T(8,128)(2,1)}, f32[512,512]{1,0:T(8,128)}) fusion(f32[512,512]{1,0:T(8,128)S(1)} %get-tuple-element.61, f32[512]{0:T(512)S(1)} %get-tuple-element.103, f32[512]{0:T(512)S(1)} %get-tuple-element.102, f32[512]{0:T(512)S(1)} %copy-done.3, ...), kind=kOutput, calls=%fused_computation.151 | convolution fusion | flops 2152462848 | bytes 11022336 | tf_op jit(solution)/shard_map/dot_general | solution.py:372
  73.0 0.0 copy-done.1
  73.0 3.7 %all_to_all.13 = f32[2,1,1024]{2,1,0:T(1,128)S(1)} all-to-all(f32[2,1,1024]{2,1,0:T(1,128)S(1)} %broadcast_in_dim.7), channel_id=1, replica_groups=mesh['sp'=64,'tp'=2] {'tp'}, dimensions={0} | all-to-all | bytes 16384 | tf_op jit(solution)/shard_map/all_to_all | solution.py:325
  76.7 4.2 %multiply_reduce_fusion.1 = (f32[512]{0:T(512)S(1)}, f32[512]{0:T(512)S(1)}, f32[512]{0:T(512)S(1)}, f32[512]{0:T(512)S(1)}, f32[512]{0:T(512)S(1)}, /*index=5*/...) fusion(f32[542,512]{1,0:T(8,128)S(1)} %maximum_convert_fusion, ...), kind=kLoop, calls=%fused_computation.152 | loop fusion | flops 11262976 | bytes 22067200 | tf_op jit(solution)/shard_map/reduce_sum | solution.py:388
  80.9 1.3 collective-permute-start.2
  82.2 4.8 %collective-permute-start.3 = (f32[15,512]{1,0:T(8,128)S(1)}, f32[15,512]{1,0:T(8,128)S(1)}, u32[]{:S(2)}, u32[]{:S(2)}) collective-permute-start(f32[15,512]{1,0:T(8,128)S(1)} %get-tuple-element.66), channel_id=1, source_target_pairs={{0,2},{2,4},{4,6},{6,8},{8,10},{10,12},{12,14},{14,16},{16,18},{18... | collective-permute-start | bytes 92168 | tf_op jit(solution)/shard_map/ppermute | solution.py:315
  87.0 2.3 %multiply_reduce_fusion.2 = (f32[512]{0:T(512)S(1)}, f32[512]{0:T(512)S(1)}, f32[512]{0:T(512)S(1)}, f32[512]{0:T(512)}, f32[512]{0:T(512)}, /*index=5*/f32[512]...) fusion(f32[512,512]{1,0:T(8,128)S(1)} %get-tuple-element.55, ...), kind=kLoop, calls=%fused_computation.153 | loop fusion | flops 6809088 | bytes 14706688 | tf_op jit(solution)/shard_map/reduce_sum | solution.py:388
  89.3 4.6 %concatenate.56.small = f32[32,512]{1,0:T(8,128)} concatenate(f32[1,512]{1,0:T(1,128)} %bitcast.161, f32[1,512]{1,0:T(1,128)} %bitcast.160, f32[1,512]{1,0:T(1,128)} %bitcast.159, f32[1,512]{1,0:T(1,128)} %bitcast.158, f32[1,512]{1,0:T(1,128)} %bitcast.157, f32[1,512]{1,0:T(1,128)} %bitcast.156, f32[1,512]{1,0:T(1,128)} %bitcast.155, f32[1,512]{1,0:T(1,128)} %bitcast.154, ...), dimensions={0} | concatenate | bytes 131072 | tf_op jit(solution)/shard_map/concatenate | solution.py:393
  94.0 0.0 collective-permute-done.2
  94.0 0.0 collective-permute-done.3
  94.0 5.8 %fusion.97 = (bf16[512,512]{1,0:T(8,128)(2,1)}, f32[512,512]{1,0:T(8,128)}, f32[512,512]{1,0:T(8,128)S(1)}) fusion(bf16[512,512]{1,0:T(8,128)(2,1)S(1)} %convolution_convert_fusion, bf16[512,512]{1,0:T(8,128)(2,1)S(1)} %convolution_convert_fusion.1, f32[512,512]{1,0:T(8,128)S(1)} %get-tuple-element.55, f32[15,512]{1,0:T(8,128)S(1)} %collective-permute-done.3, ...), kind=kLoop, calls=%fused_computation.204 | loop fusion | flops 26476544 | bytes 4843520 | tf_op jit(solution)/shard_map/convert_element_type | solution.py:392
  99.8 1.5 fusion.100
  101.2 84.3 %shard_map.126 = (f32[64,512]{1,0:T(8,128)}, f32[64,512]{1,0:T(8,128)}, f32[64,512]{1,0:T(8,128)}, f32[32,512]{1,0:T(8,128)}) custom-call(bf16[512,4096]{1,0:T(8,128)(2,1)} %get-tuple-element.63.feat, bf16[512,4096]{1,0:T(8,128)(2,1)} %get-tuple-element.62.cot, bf16[512,512]{1,0:T(8,128)(2,1)} %get-tuple-element.64.act, ...), custom_call_target="tpu_custom_call" | custom-call | tf_op jit(solution)/shard_map/pallas_call | solution.py:280
  185.6 1.3 slice.499
  186.9 1.6 copy.26
  188.5 1.6 copy.27
  190.0 1.6 copy.28
  191.6 1.5 copy.29
  (12 shorter events, 0.1 us)
Async XLA Ops:
  7.2 30.0 %all-gather.2.cloned.1.call-start = ((), (), s32[]{:S(2)}) async-start(), calls=%async_computation.2 | async-start | bytes 12582912 | tf_op jit(solution)/shard_map/all_gather | solution.py:307
  12.0 0.8 copy-start.2
  37.2 5.9 %copy-start = (bf16[1024,4096]{1,0:T(8,128)(2,1)S(1)}, bf16[1024,4096]{1,0:T(8,128)(2,1)}, u32[]{:S(2)}) copy-start(bf16[1024,4096]{1,0:T(8,128)(2,1)} %all-gather.2.cloned.1.call-done) | copy-start | bytes 25165828
  37.2 7.0 %copy-start.4 = (bf16[4096,512]{1,0:T(8,128)(2,1)S(1)}, bf16[4096,512]{1,0:T(8,128)(2,1)}, u32[]{:S(2)}) copy-start(bf16[4096,512]{1,0:T(8,128)(2,1)} %param.8) | copy-start | bytes 12582916
  46.9 8.5 %collective-permute-start = (bf16[15,512]{1,0:T(8,128)(2,1)S(1)}, bf16[15,512]{1,0:T(8,128)(2,1)S(1)}, u32[]{:S(2)}, u32[]{:S(2)}) collective-permute-start(bf16[15,512]{1,0:T(8,128)(2,1)S(1)} %get-tuple-element.67), channel_id=1, source_target_pairs={{0,2},{2,4},{4,6},{6,8},{8,10},{10,12},{12,14},{14,16},{16,18},{18... | collective-permute-start | bytes 46088 | tf_op jit(solution)/shard_map/ppermute | solution.py:315
  50.4 5.6 %collective-permute-start.1 = (bf16[15,512]{1,0:T(8,128)(2,1)S(1)}, bf16[15,512]{1,0:T(8,128)(2,1)S(1)}, u32[]{:S(2)}, u32[]{:S(2)}) collective-permute-start(bf16[15,512]{1,0:T(8,128)(2,1)S(1)} %get-tuple-element.68), channel_id=1, source_target_pairs={{2,0},{4,2},{6,4},{8,6},{10,8},{12,10},{14,12},{16,14},{18,16},{20... | collective-permute-start | bytes 46088 | tf_op jit(solution)/shard_map/ppermute | solution.py:318
  56.2 8.9 %copy-start.3 = (f32[512]{0:T(512)S(1)}, f32[512]{0:T(512)}, u32[]{:S(2)}) copy-start(f32[512]{0:T(512)} %param.12) | copy-start | bytes 6148
  61.2 11.7 %copy-start.1 = (f32[512,512]{1,0:T(8,128)}, f32[512,512]{1,0:T(8,128)S(1)}, u32[]{:S(2)}) copy-start(f32[512,512]{1,0:T(8,128)S(1)} %get-tuple-element.61) | copy-start | bytes 3145732
  80.9 13.0 %collective-permute-start.2 = (f32[15,512]{1,0:T(8,128)S(1)}, f32[15,512]{1,0:T(8,128)S(1)}, u32[]{:S(2)}, u32[]{:S(2)}) collective-permute-start(f32[15,512]{1,0:T(8,128)S(1)} %get-tuple-element.65), channel_id=1, source_target_pairs={{2,0},{4,2},{6,4},{8,6},{10,8},{12,10},{14,12},{16,14},{18,16},{20... | collective-permute-start | bytes 92168 | tf_op jit(solution)/shard_map/ppermute | solution.py:318
  82.2 11.7 %collective-permute-start.3 = (f32[15,512]{1,0:T(8,128)S(1)}, f32[15,512]{1,0:T(8,128)S(1)}, u32[]{:S(2)}, u32[]{:S(2)}) collective-permute-start(f32[15,512]{1,0:T(8,128)S(1)} %get-tuple-element.66), channel_id=1, source_target_pairs={{0,2},{2,4},{4,6},{6,8},{8,10},{10,12},{12,14},{14,16},{16,18},{18... | collective-permute-start | bytes 92168 | tf_op jit(solution)/shard_map/ppermute | solution.py:315
Sparse Core Ops, SparseCore 0:
  12.1 25.0 all-gather.1

commit v3 on v2

v3 whole, which is shorter than its diff:
```python
import functools

import jax
import jax.numpy as jnp
from jax import lax
from jax.experimental import pallas as pl
from jax.experimental.pallas import tpu as pltpu
from jax.sharding import PartitionSpec as P

SP = "sp"
MESH = pl.DeviceIdType.MESH
BF16 = jnp.bfloat16
F32 = jnp.float32

NORM_EPS = 1e-05

WIDTHS = ((128, 128, 256), (256, 128, 128), (128, 256, 128))
ORDERS = ("xzy", "yxz", "zyx")
ROWS = (512, 128, 32)
SENT = (BF16, BF16, F32)


def coords():
    sp = lax.axis_index("sp")
    return {"z": sp // 16, "y": (sp // 4) % 4, "x": sp % 4}


def peer(where, dim, shift):
    to = dict(where)
    to[dim] = (where[dim] + shift + 4) % 4
    return (to["z"] * 16 + to["y"] * 4 + to["x"], lax.axis_index("tp"))


def remote(src, dst, ssem, rsem, device):
    return pltpu.make_async_remote_copy(
        src_ref=src, dst_ref=dst, send_sem=ssem, recv_sem=rsem,
        device_id=device, device_id_type=MESH,
    )


class Part:
    def __init__(self, where, p, lhs_t, rhs, cols, out, bufs, sems):
        self.where, self.p, self.lhs_t, self.rhs = where, p, lhs_t, rhs
        self.cols, self.out, self.bufs, self.sems = cols, out, bufs, sems

    def source(self, stage, h, j):
        off, width = self.cols
        if stage == 0:
            if self.p == 0:
                rows = self.lhs_t[pl.ds(2 * h, 2), :, j]
            elif self.p == 1:
                rows = self.lhs_t[:, j, pl.ds(2 * h, 2)]
            else:
                rows = self.lhs_t[j, pl.ds(2 * h, 2)]
            rows = rows.reshape(512, rows.shape[-1])
            return jnp.dot(rows, self.rhs[:, off : off + width], preferred_element_type=F32)
        held = self.bufs[stage - 1][2]
        if stage == 1:
            if self.p == 1:
                at = (j // 2) * 8 + j % 2
                two = [held[at + 2 * (2 * h + i)] for i in range(2)]
                return jnp.concatenate(two, axis=0)
            return held[pl.ds(4 * j + 2 * h, 2)].reshape(128, width)
        return held[j, pl.ds(pl.multiple_of(h * 32, 32), 32)]

    def place(self, stage, h, value):
        off, width = self.cols
        if stage == 2:
            self.out[pl.ds(pl.multiple_of(h * 32, 32), 32), off : off + width] = value
            return
        held = self.bufs[stage][2]
        count = ROWS[stage] // 64
        held[pl.ds(count * h, count)] = value.reshape(count, 64, width)

    def copy(self, stage, slot, sign):
        send, recv, _ = self.bufs[stage]
        ssem, rsem = self.sems
        at = stage * 6 + slot
        dim = ORDERS[self.p][stage]
        return remote(
            send.at[slot], recv.at[slot], ssem.at[at], rsem.at[at],
            peer(self.where, dim, sign),
        )

    def first(self, stage):
        m = self.where[ORDERS[self.p][stage]]
        send = self.bufs[stage][0]

        @pl.loop(0, 4)
        def _(i):
            sign = 1 - 2 * (i % 2)
            h = ((i + 1) // 2) % 2
            j = (m + 6 - (i // 2) * sign) % 4
            send[i] = self.source(stage, h, j).astype(SENT[stage])
            self.copy(stage, i, sign).start()

    def second(self, stage):
        m = self.where[ORDERS[self.p][stage]]
        send, recv, _ = self.bufs[stage]

        @pl.loop(0, 2)
        def _(k):
            sign = 1 - 2 * k
            self.copy(stage, k, sign).wait_recv()
            mine = self.source(stage, k, (m + 4 + sign) % 4)
            send[4 + k] = (mine + recv[k].astype(F32)).astype(SENT[stage])
            self.copy(stage, 4 + k, sign).start()

    def third(self, stage):
        m = self.where[ORDERS[self.p][stage]]
        recv = self.bufs[stage][1]

        @pl.loop(0, 2)
        def _(h):
            mine = self.source(stage, h, m)
            self.copy(stage, 3 - h, 1).wait_recv()
            self.copy(stage, 4 + h, 1).wait_recv()
            total = mine + recv[3 - h].astype(F32) + recv[4 + h].astype(F32)
            self.place(stage, h, total)

    def drain(self, stage):
        @pl.loop(0, 6)
        def _(slot):
            self.copy(stage, slot, 1).wait_send()


class Small:
    def __init__(self, where, cols, slots, sums, out, sems):
        self.where, self.cols, self.slots = where, cols, slots
        self.sums, self.out, self.sems = sums, out, sems

    def copy(self, stage, d):
        dim = "xyzx"[stage]
        mine = self.where[dim]
        ssem, rsem = self.sems
        src = self.cols.at[(mine + d) % 4] if stage == 0 else self.sums.at[stage - 1]
        at = stage * 4 + d
        return remote(src, self.slots.at[stage, mine], ssem.at[at], rsem.at[at],
                      peer(self.where, dim, d))

    def send(self, stage):
        mine = self.where["xyzx"[stage]]
        if stage == 0:
            self.slots[0, mine] = self.cols[mine]
        else:
            self.slots[stage, mine] = self.sums[stage - 1]

        @pl.loop(1, 4)
        def _(d):
            self.copy(stage, d).start()

    def collect(self, stage):
        @pl.loop(1, 4)
        def _(d):
            self.copy(stage, d).wait_recv()

        if stage < 3:
            a, b, c, d = [self.slots[stage, j] for j in range(4)]
            self.sums[stage] = (a + b) + (c + d)
        else:
            for j in range(4):
                self.out[:, 128 * j : 128 * j + 128] = self.slots[3, j]

    def drain(self):
        for stage in range(4):
            @pl.loop(1, 4)
            def _(d):
                self.copy(stage, d).wait_send()


def greet(where):
    barrier = pltpu.get_barrier_semaphore()
    for to in others(where):
        pl.semaphore_signal(barrier, inc=1, device_id=to, device_id_type=MESH)
    pl.semaphore_wait(barrier, 12)


def partner():
    return (lax.axis_index("sp"), 1 - lax.axis_index("tp"))


def along(shift):
    return ((lax.axis_index("sp") + 64 + shift) % 64, lax.axis_index("tp"))


def others(where):
    near = [peer(where, dim, shift) for dim in "zyx" for shift in (1, 2, 3)]
    return near + [along(-1), along(1), partner()]


AGAIN = {(2, 0): (0, 0), (2, 1): (0, 2), (2, 2): (0, 1)}


def part_scratch():
    shapes = []
    for r, widths in enumerate(WIDTHS):
        for p, width in enumerate(widths):
            for stage in range(3):
                shape = pltpu.VMEM((6, ROWS[stage], width), SENT[stage])
                shapes.append(shape)
                if (r, p) not in AGAIN:
                    shapes.append(shape)
                if stage < 2:
                    shapes.append(pltpu.VMEM((ROWS[stage] // 32, 64, width), F32))
            shapes.append(pltpu.SemaphoreType.DMA((18,)))
            shapes.append(pltpu.SemaphoreType.DMA((18,)))
    return shapes


def take_parts(where, r, lhs_t, rhs, out, pool, earlier):
    parts, off = [], 0
    for p, width in enumerate(WIDTHS[r]):
        bufs = []
        for stage in range(3):
            recv = next(pool)
            if (r, p) in AGAIN:
                r0, p0 = AGAIN[(r, p)]
                send = earlier[r0][p0].bufs[stage][0]
            else:
                send = next(pool)
            bufs.append((send, recv, next(pool) if stage < 2 else None))
        sems = (next(pool), next(pool))
        parts.append(Part(where, p, lhs_t, rhs, (off, width), out, bufs, sems))
        off += width
    return parts


def flip(src, dst, h, k):
    for q in range(2):
        at = pl.multiple_of(k * 512 + q * 256, 256)
        cols = src[h, :, pl.ds(at, 256)]
        dst[h * 2 + k // 2, (k % 2) * 2 + q] = cols.T.reshape(4, 64, 512)


def lane_sum(a):
    return jnp.sum(a, axis=-1, keepdims=True)


def fold(a):
    return jnp.sum(a.reshape(-1, 8, 128), axis=0)


def whole_kernel(
    feat_hbm, wv_hbm, wg_hbm, wo_hbm, taps_in, gain_in, cot_hbm,
    vgrad_hbm, ggrad_hbm, value_out, gate_out, out_out, small_out,
    feat, cot, feat_t, cot_t, wbuf, wobuf, acc0, acc1, acc2, vhalf, ghalf,
    ext, gext, taps, gains, act, vlow, glow, edges, edges_in, gedges, gedges_in,
    stats, stats_in, inv_rows, cols, slots, sums,
    w_sem, wo_sem, f_sem, f_ssem, f_rsem, c_sem, c_ssem, c_rsem,
    e_ssem, e_rsem, s_ssem, s_rsem, o_sem, small_ssem, small_rsem, *pool,
):
    where = coords()
    sp, tp = lax.axis_index("sp"), lax.axis_index("tp")
    pool = iter(pool)
    tiny = Small(where, cols, slots, sums, small_out, (small_ssem, small_rsem))
    out_parts = take_parts(where, 0, cot_t, act, out_out, pool, ())
    value_parts = take_parts(where, 1, feat_t, vlow, value_out, pool, ())
    gate_parts = take_parts(where, 2, feat_t, glow, gate_out, pool, (out_parts,))

    def run(name, parts, stage):
        for part in parts:
            getattr(part, name)(stage)

    def half_of(k):
        return (tp + k // 4) % 2

    def w_loads(k):
        row = pl.multiple_of(half_of(k) * 2048 + (k % 4) * 512, 512)
        slot = k % 3
        return [
            pltpu.make_async_copy(w.at[pl.ds(row, 512)], wbuf.at[slot, i], w_sem.at[slot, i])
            for i, w in enumerate((wv_hbm, wg_hbm))
        ]

    def wo_load(k):
        row = pl.multiple_of(half_of(k) * 2048 + (k % 4) * 512, 512)
        slot = k % 3
        return pltpu.make_async_copy(wo_hbm.at[pl.ds(row, 512)], wobuf.at[slot], wo_sem.at[slot])

    def cut(k):
        return pl.ds(pl.multiple_of(k * 512, 512), 512)

    def own(src, dst, sem, k):
        return pltpu.make_async_copy(src.at[:, cut(k)], dst.at[tp, :, cut(k)], sem.at[k])

    def give(src, dst, ssem, rsem, k):
        return remote(
            src.at[:, cut(k)], dst.at[tp, :, cut(k)], ssem.at[k], rsem.at[k], partner()
        )

    for k in range(2):
        own(feat_hbm, feat, f_sem, k).start()
        for c in w_loads(k):
            c.start()
    greet(where)
    for k in range(4):
        give(feat_hbm, feat, f_ssem, f_rsem, k).start()
    for k in range(2, 4):
        own(feat_hbm, feat, f_sem, k).start()
    for c in w_loads(2):
        c.start()
    for k in range(4):
        give(cot_hbm, cot, c_ssem, c_rsem, k).start()
    for k in range(4):
        own(cot_hbm, cot, c_sem, k).start()
    for k in range(3):
        wo_load(k).start()

    acc0[...] = jnp.zeros_like(acc0)
    acc1[...] = jnp.zeros_like(acc1)
    acc2[...] = jnp.zeros_like(acc2)
    for c in range(4):
        taps[c, 0:31] = taps_in[:, 128 * c : 128 * c + 128]
        gains[c] = jnp.broadcast_to(gain_in[:, 128 * c : 128 * c + 128], (8, 128))

    def add_dot(acc, x, w):
        for c in range(2):
            got = jnp.dot(x, w[:, 256 * c : 256 * c + 256], preferred_element_type=F32)
            acc[2 * c] += got[:, :128]
            acc[2 * c + 1] += got[:, 128:]

    def project(lo, arrived):
        @pl.loop(lo, lo + 4)
        def _(k):
            for c in w_loads(k):
                c.wait()
            arrived(k - lo)
            x = feat[half_of(k), :, cut(k % 4)]
            for i, acc in enumerate((acc0, acc1)):
                add_dot(acc, x, wbuf[k % 3, i])

            @pl.when(k + 3 < 8)
            def _():
                for c in w_loads(k + 3):
                    c.start()

    project(0, lambda k: own(feat_hbm, feat, f_sem, k).wait())
    project(4, lambda k: give(feat_hbm, feat, f_ssem, f_rsem, k).wait_recv())

    def gate_rows(at):
        kept = []
        for c in range(4):
            value = acc0[c, pl.ds(at, 32)].astype(BF16)
            gate = acc1[c, pl.ds(at, 32)].astype(BF16)
            vhalf[c, pl.ds(at, 32)] = value
            ghalf[c, pl.ds(at, 32)] = gate
            sig = jax.nn.sigmoid(gate.astype(F32))
            mixed = (value.astype(F32) * sig).astype(BF16)
            ext[c, pl.ds(at + 16, 32)] = mixed.astype(F32)
            kept.append(mixed)
        return kept

    def edge(send, recv, i, at):
        return remote(send.at[i], recv.at[i], e_ssem.at[at + i], e_rsem.at[at + i],
                      along(2 * i - 1))

    for i, kept in enumerate((gate_rows(0), gate_rows(480))):
        for c in range(4):
            edges[i, c] = kept[c][16 * i : 16 * i + 16]
    for i in range(2):
        edge(edges, edges_in, i, 0).start()

    @pl.loop(1, 15)
    def _(b):
        gate_rows(pl.multiple_of(b * 32, 32))

    def cot_step(lo, arrived):
        @pl.loop(lo, lo + 4)
        def _(k):
            wo_load(k).wait()
            arrived(k - lo)
            h = half_of(k)
            add_dot(acc2, cot[h, :, cut(k % 4)], wobuf[k % 3])
            flip(cot, cot_t, h, k % 4)

            @pl.when(k + 3 < 8)
            def _():
                wo_load(k + 3).start()

    cot_step(0, lambda k: own(cot_hbm, cot, c_sem, k).wait())
    cot_step(4, lambda k: give(cot_hbm, cot, c_ssem, c_rsem, k).wait_recv())

    def fill(buf, got, i):
        inside = sp > 0 if i == 0 else sp < 63
        for c in range(4):
            rows = got[1 - i, c].astype(F32)
            buf[c, 528 * i : 528 * i + 16] = jnp.where(inside, rows, 0.0)

    for i in range(2):
        edge(edges, edges_in, 1 - i, 0).wait_recv()
        fill(ext, edges_in, i)

    def conv(buf, c, at, first, step):
        total = jnp.zeros((64, 128), F32)
        for k in range(31):
            rows = buf[c, pl.ds(at + (first + step * k), 64)]
            total = total + taps[c, k : k + 1] * rows
        return total

    def share(n):
        return remote(stats.at[n], stats_in.at[n], s_ssem.at[n], s_rsem.at[n], partner())

    @pl.loop(0, 8)
    def _(b):
        at = pl.multiple_of(b * 64, 64)
        zero = jnp.zeros((64, 128), F32)

        @pl.loop(0, 4, init_carry=(zero, zero))
        def totals(c, carry):
            got = conv(ext, c, at, 1, 1)
            acc0[c, pl.ds(at, 64)] = got
            return carry[0] + got, carry[1] + got * got

        stats[0, 0, pl.ds(at, 64)] = totals[0]
        stats[0, 1, pl.ds(at, 64)] = totals[1]

    share(0).start()

    @pl.loop(0, 4)
    def _(k):
        flip(feat, feat_t, tp, k)

    share(0).wait_recv()

    none = jnp.zeros((8, 128), F32)

    @pl.loop(0, 16, init_carry=(none,) * 4)
    def gain_sums(b, carry):
        at = pl.multiple_of(b * 32, 32)
        rows = pl.ds(at, 32)
        mean = lane_sum(stats[0, 0, rows] + stats_in[0, 0, rows]) / 1024
        square = lane_sum(stats[0, 1, rows] + stats_in[0, 1, rows]) / 1024
        inv = lax.rsqrt(square - mean * mean + NORM_EPS)
        inv_rows[rows] = jnp.broadcast_to(inv, (32, 128))
        first = jnp.zeros((32, 128), F32)
        second = jnp.zeros((32, 128), F32)
        carried = []
        for c in range(4):
            gain = gains[c, 0:1]
            normed = (acc0[c, rows] - mean) * inv
            pre = normed * gain
            sig = jax.nn.sigmoid(pre)
            act[rows, 128 * c : 128 * c + 128] = (pre * sig).astype(BF16)
            grad = acc2[c, rows] * sig * (1.0 + pre * (1.0 - sig))
            carried.append(carry[c] + fold(grad * normed))
            ngrad = grad * gain
            acc0[c, rows] = normed
            acc1[c, rows] = ngrad
            first = first + ngrad
            second = second + ngrad * normed
        stats[1, 0, rows] = first
        stats[1, 1, rows] = second
        return tuple(carried)

    share(1).start()
    for c in range(4):
        cols[c, 31:32] = jnp.sum(gain_sums[c], axis=0, keepdims=True)
    run("first", out_parts, 0)
    share(1).wait_recv()

    def conv_grad(at):
        rows = pl.ds(at, 32)
        m1 = lane_sum(stats[1, 0, rows] + stats_in[1, 0, rows]) / 1024
        m2 = lane_sum(stats[1, 1, rows] + stats_in[1, 1, rows]) / 1024
        kept = []
        for c in range(4):
            got = inv_rows[rows] * (acc1[c, rows] - m1 - acc0[c, rows] * m2)
            gext[c, pl.ds(at + 16, 32)] = got
            kept.append(got)
        return kept

    for i, kept in enumerate((conv_grad(0), conv_grad(480))):
        for c in range(4):
            gedges[i, c] = kept[c][16 * i : 16 * i + 16]
    for i in range(2):
        edge(gedges, gedges_in, i, 2).start()

    @pl.loop(1, 15)
    def _(b):
        conv_grad(pl.multiple_of(b * 32, 32))

    run("second", out_parts, 0)

    @pl.loop(0, 4)
    def _(c):
        @pl.loop(0, 64, init_carry=(none,) * 31)
        def tap_sums(b, carry):
            at = pl.multiple_of(b * 8, 8)
            grad = gext[c, pl.ds(at + 16, 8)]
            return tuple(
                carry[k] + grad * ext[c, pl.ds(at + (k + 1), 8)] for k in range(31)
            )

        for k in range(31):
            cols[c, k : k + 1] = jnp.sum(tap_sums[k], axis=0, keepdims=True)

    tiny.send(0)

    @pl.loop(0, 4)
    def _(k):
        flip(feat, feat_t, 1 - tp, k)

    for i in range(2):
        edge(gedges, gedges_in, 1 - i, 2).wait_recv()
        fill(gext, gedges_in, i)

    @pl.loop(0, 8)
    def _(b):
        at = pl.multiple_of(b * 64, 64)
        rows = pl.ds(at, 64)

        @pl.loop(0, 4)
        def _(c):
            mixed_grad = conv(gext, c, at, 31, -1)
            value = vhalf[c, rows].astype(F32)
            sig = jax.nn.sigmoid(ghalf[c, rows].astype(F32))
            vgrad = mixed_grad * sig
            ggrad = mixed_grad * value * sig * (1.0 - sig)
            acc0[c, rows] = vgrad
            acc1[c, rows] = ggrad
            lanes = pl.ds(pl.multiple_of(c * 128, 128), 128)
            vlow[rows, lanes] = vgrad.astype(BF16)
            glow[rows, lanes] = ggrad.astype(BF16)

    def store(i, c):
        src, dst = ((acc0, vgrad_hbm), (acc1, ggrad_hbm))[i]
        return pltpu.make_async_copy(
            src.at[c], dst.at[:, 128 * c : 128 * c + 128], o_sem.at[i, c]
        )

    for i in range(2):
        for c in range(4):
            store(i, c).start()

    run("first", value_parts, 0)
    for part in out_parts:
        part.drain(0)
    run("first", gate_parts, 0)
    run("third", out_parts, 0)
    run("first", out_parts, 1)
    tiny.collect(0)
    tiny.send(1)
    run("second", value_parts, 0)
    run("second", gate_parts, 0)
    run("second", out_parts, 1)
    tiny.collect(1)
    tiny.send(2)
    run("third", value_parts, 0)
    run("first", value_parts, 1)
    run("third", out_parts, 1)
    run("first", out_parts, 2)
    tiny.collect(2)
    tiny.send(3)
    for part in out_parts:
        part.drain(1)
    run("third", gate_parts, 0)
    run("first", gate_parts, 1)
    run("second", value_parts, 1)
    run("second", out_parts, 2)
    run("second", gate_parts, 1)
    run("third", out_parts, 2)
    for part in out_parts:
        part.drain(2)
    run("third", value_parts, 1)
    run("first", value_parts, 2)
    run("third", gate_parts, 1)
    run("first", gate_parts, 2)
    run("second", value_parts, 2)
    run("second", gate_parts, 2)
    tiny.collect(3)
    run("third", value_parts, 2)
    run("third", gate_parts, 2)

    tiny.drain()
    for part in (*value_parts, *gate_parts):
        for stage in range(3):
            part.drain(stage)
    for k in range(4):
        give(feat_hbm, feat, f_ssem, f_rsem, k).wait_send()
        give(cot_hbm, cot, c_ssem, c_rsem, k).wait_send()
    for i in range(2):
        edge(edges, edges_in, i, 0).wait_send()
        edge(gedges, gedges_in, i, 2).wait_send()
        share(i).wait_send()
        for c in range(4):
            store(i, c).wait()


def on_device(features, weight_value, weight_gate, weight_out, conv_taps, norm_gain, out_grad):
    grad = jax.ShapeDtypeStruct((512, 512), F32)
    piece = jax.ShapeDtypeStruct((64, 512), F32)
    vmem = pl.BlockSpec(memory_space=pltpu.VMEM)
    hbm = pl.BlockSpec(memory_space=pl.ANY)
    dma = pltpu.SemaphoreType.DMA
    tiles = (4, 512, 128)
    vgrad, ggrad, vw, gw, ow, small = pl.pallas_call(
        whole_kernel,
        out_shape=(grad, grad, piece, piece, piece, jax.ShapeDtypeStruct((32, 512), F32)),
        in_specs=[hbm, hbm, hbm, hbm, vmem, vmem, hbm],
        out_specs=(hbm, hbm, vmem, vmem, vmem, vmem),
        scratch_shapes=[
            pltpu.VMEM((2, 512, 2048), BF16),
            pltpu.VMEM((2, 512, 2048), BF16),
            pltpu.VMEM((4, 4, 4, 64, 512), BF16),
            pltpu.VMEM((4, 4, 4, 64, 512), BF16),
            pltpu.VMEM((3, 2, 512, 512), BF16),
            pltpu.VMEM((3, 512, 512), BF16),
            pltpu.VMEM(tiles, F32),
            pltpu.VMEM(tiles, F32),
            pltpu.VMEM(tiles, F32),
            pltpu.VMEM(tiles, BF16),
            pltpu.VMEM(tiles, BF16),
            pltpu.VMEM((4, 544, 128), F32),
            pltpu.VMEM((4, 544, 128), F32),
            pltpu.VMEM((4, 32, 128), F32),
            pltpu.VMEM((4, 8, 128), F32),
            pltpu.VMEM((512, 512), BF16),
            pltpu.VMEM((512, 512), BF16),
            pltpu.VMEM((512, 512), BF16),
            pltpu.VMEM((2, 4, 16, 128), BF16),
            pltpu.VMEM((2, 4, 16, 128), BF16),
            pltpu.VMEM((2, 4, 16, 128), F32),
            pltpu.VMEM((2, 4, 16, 128), F32),
            pltpu.VMEM((2, 2, 512, 128), F32),
            pltpu.VMEM((2, 2, 512, 128), F32),
            pltpu.VMEM((512, 128), F32),
            pltpu.VMEM((4, 32, 128), F32),
            pltpu.VMEM((4, 4, 32, 128), F32),
            pltpu.VMEM((3, 32, 128), F32),
            dma((3, 2)), dma((3,)),
            dma((4,)), dma((4,)), dma((4,)),
            dma((4,)), dma((4,)), dma((4,)),
            dma((4,)), dma((4,)), dma((2,)), dma((2,)), dma((2, 4)),
            dma((16,)), dma((16,)),
            *part_scratch(),
        ],
        compiler_params=pltpu.CompilerParams(
            collective_id=0, has_side_effects=True, vmem_limit_bytes=64 * 1024 * 1024 - 65536
        ),
    )(features, weight_value, weight_gate, weight_out, conv_taps, norm_gain[None], out_grad)
    return vgrad, ggrad, vw, gw, ow, small[:31], small[31]


def solution(mesh):
    return jax.shard_map(
        on_device,
        mesh=mesh,
        in_specs=(
            P(SP, "tp"), P(None, "tp"), P(None, "tp"), P(None, "tp"),
            P(None, "tp"), P("tp"), P(SP, "tp"),
        ),
        out_specs=(
            P(SP, "tp"), P(SP, "tp"), P(SP, "tp"), P(SP, "tp"), P(SP, "tp"),
            P(None, "tp"), P("tp"),
        ),
        check_vma=False,
    )
```

time: 200 us -> 117 us (0.58)
  waiting for transfers between devices: 24.9 us -> 0 us
  other arithmetic: 24.1 us -> 0 us
  Pallas kernels: 84.3 us -> 107 us
  matrix products: 16.2 us -> 0 us
  between operations: 14.2 us -> 0.68 us
  starting transfers between devices: 10.9 us -> 0 us
  local copies, waits for them, and re-layouts: 17.8 us -> 8.5 us
  blocking collectives: 7.42 us -> 0 us
    all_gather x1 -> x0, waiting for transfers between devices: 24.3 us -> none  [in_one_piece(): lax.all_gather(both, axis, axis=dim, tiled=True)]
    pallas_call x1, Pallas kernels: 84.3 us -> 107 us  [on_device(): pl.pallas_call(whole_kernel, out_shape=(grad, grad, piece, piece, piece,...]
    dot_general x3 -> x0, matrix products: 16.2 us -> none  [the longest x1 7.93 us: on_device(): jnp.dot(whole_cotangent, weight_out, preferred_element_type=jnp.float32)]
    reduce_sum x5 -> x0, other arithmetic: 11.6 us -> none  [the longest x2 6.51 us: on_device(): jnp.sum(conv_grad * extended[offset:offset + row_count], axis=0)]
    ppermute x4 -> x0, starting transfers between devices: 10.8 us -> none  [the longest x2 8.25 us: with_halo(): lax.ppermute(lax.slice_in_dim(block, block.shape[dim] - width, None, axis...]
    convert_element_type x4 -> x0, other arithmetic: 7.7 us -> none  [the longest x1 5.81 us: on_device(): gate_low = gate_grad.astype(jnp.bfloat16)]
    all_to_all x2 -> x0, blocking collectives: 7.42 us -> none  [from_everyone(): lax.all_to_all(jnp.broadcast_to(x[None], (devices, *x.shape)), axis, 0, 0...]
    concatenate x3 -> x0, other arithmetic: 4.8 us -> none  [the longest x1 4.79 us: in_one_piece(): both = jnp.concatenate(arrays, axis=along)]
  transfers between devices with their start and end apart: 5 -> 0, of which waited for: 2 -> 0; matrix products, arithmetic and copies ran while one was open for 5% -> 0% of each run, Pallas kernels for 0% -> 0%
where the time goes in v3:
time: 117 us; the launch traced here: 116 us
  Pallas kernels  107 us (91%)
  local copies, waits for them, and re-layouts  8.5 us (7%)
    pallas_call x1, Pallas kernels, on_device(): pl.pallas_call(whole_kernel, out_shape=(grad, grad, piece, piece, piece,...  107 us
    unnamed x14, local copies, waits for them, and re-layouts  7.14 us

profile of v3, /device:TPU:0, one launch (start us, length us, event | category | flops | bytes accessed | tf_op | source)
XLA Modules:
  0.0 116.5 jit_solution(17603519175185955927)
XLA Ops:
  0.6 107.3 %shard_map.126 = (f32[512,512]{1,0:T(8,128)}, f32[512,512]{1,0:T(8,128)}, f32[64,512]{1,0:T(8,128)}, f32[64,512]{1,0:T(8,128)}, f32[64,512]{1,0:T(8,128)}, /*index=5*/f32[32,512]{1,0:T(8,128)}) custom-call(bf16[512,2048]{1,0:T(8,128)(2,1)} %feat_hbm.1, bf16[4096,512]{1,0:T(8,128)(2,1)} %wv_hbm.1, bf16[4096,512]{1,0:T(8,128)(2,1)} %wg_hbm.1, ...), custom_call_target="tpu_custom_call" | custom-call | tf_op jit(solution)/shard_map/pallas_call | solution.py:596
  107.9 0.0 copy-start.2
  107.9 0.0 copy-start.1
  108.0 0.0 copy-start
  108.0 0.0 copy-start.3
  108.0 1.4 %slice.7 = f32[1,512]{1,0:T(1,128)} slice(f32[32,512]{1,0:T(8,128)} %get-tuple-element.18), slice={[31:32], [0:512]} | slice | bytes 4096 | tf_op jit(solution)/shard_map/slice | solution.py:641
  109.3 2.3 %copy.20 = f32[512,512]{1,0:T(8,128)} copy(f32[512,512]{1,0:T(8,128)} %get-tuple-element.26) | data formatting | bytes 2097152
  111.6 2.3 %copy.21 = f32[512,512]{1,0:T(8,128)} copy(f32[512,512]{1,0:T(8,128)} %get-tuple-element.27) | data formatting | bytes 2097152
  113.9 0.0 copy-done.2
  113.9 0.7 copy.22
  114.5 0.0 copy-done.1
  114.5 0.7 copy.23
  115.2 0.0 copy-done
  115.2 0.7 copy.24
  115.8 0.0 copy-done.3
  115.8 0.6 copy.25
Async XLA Ops:
  107.9 5.9 %copy-start.2 = (f32[64,512]{1,0:T(8,128)S(1)}, f32[64,512]{1,0:T(8,128)}, u32[]{:S(2)}) copy-start(f32[64,512]{1,0:T(8,128)} %get-tuple-element.28) | copy-start | bytes 393220
  107.9 6.6 %copy-start.1 = (f32[64,512]{1,0:T(8,128)S(1)}, f32[64,512]{1,0:T(8,128)}, u32[]{:S(2)}) copy-start(f32[64,512]{1,0:T(8,128)} %get-tuple-element.29) | copy-start | bytes 393220
  108.0 7.2 %copy-start = (f32[64,512]{1,0:T(8,128)S(1)}, f32[64,512]{1,0:T(8,128)}, u32[]{:S(2)}) copy-start(f32[64,512]{1,0:T(8,128)} %get-tuple-element.30) | copy-start | bytes 393220
  108.0 7.9 %copy-start.3 = (f32[32,512]{1,0:T(8,128)S(1)}, f32[32,512]{1,0:T(8,128)}, u32[]{:S(2)}) copy-start(f32[32,512]{1,0:T(8,128)} %get-tuple-element.18) | copy-start | bytes 196612

commit v4 on v3

--- a/solution.py
+++ b/solution.py
@@ -39,9 +39,9 @@
 
 
 class Part:
-    def __init__(self, where, p, lhs_t, rhs, cols, out, bufs, sems):
+    def __init__(self, where, p, lhs_t, rhs, cols, out, bufs, sems, spare):
         self.where, self.p, self.lhs_t, self.rhs = where, p, lhs_t, rhs
-        self.cols, self.out, self.bufs, self.sems = cols, out, bufs, sems
+        self.cols, self.out, self.bufs, self.sems, self.spare = cols, out, bufs, sems, spare
 
     def source(self, stage, h, j):
         off, width = self.cols
@@ -72,39 +72,48 @@
         count = ROWS[stage] // 64
         held[pl.ds(count * h, count)] = value.reshape(count, 64, width)
 
-    def copy(self, stage, slot, sign):
-        send, recv, _ = self.bufs[stage]
+    def sender(self, stage, slot):
+        send = self.bufs[stage][0]
+        if send is not None:
+            return send.at[slot]
+        off, width = self.cols
+        lanes = pl.ds(pl.multiple_of((slot % 3) * 512 + off, 128), width)
+        return self.spare.at[slot // 3, :, lanes]
+
+    def copy(self, stage, slot, sem, sign):
+        recv = self.bufs[stage][1]
         ssem, rsem = self.sems
-        at = stage * 6 + slot
-        dim = ORDERS[self.p][stage]
         return remote(
-            send.at[slot], recv.at[slot], ssem.at[at], rsem.at[at],
-            peer(self.where, dim, sign),
+            recv.at[slot] if isinstance(slot, pl.Slice) else self.sender(stage, slot),
+            recv.at[slot], ssem.at[stage], rsem.at[stage * 4 + sem],
+            peer(self.where, ORDERS[self.p][stage], sign),
         )
 
     def first(self, stage):
         m = self.where[ORDERS[self.p][stage]]
-        send = self.bufs[stage][0]
 
         @pl.loop(0, 4)
         def _(i):
             sign = 1 - 2 * (i % 2)
             h = ((i + 1) // 2) % 2
             j = (m + 6 - (i // 2) * sign) % 4
-            send[i] = self.source(stage, h, j).astype(SENT[stage])
-            self.copy(stage, i, sign).start()
+            slot = i + (i // 2) * (2 - 3 * (i % 2))
+            self.sender(stage, slot)[...] = self.source(stage, h, j).astype(SENT[stage])
+            self.copy(stage, slot, i + (i // 2) * sign, sign).start()
 
     def second(self, stage):
         m = self.where[ORDERS[self.p][stage]]
-        send, recv, _ = self.bufs[stage]
+        recv = self.bufs[stage][1]
 
         @pl.loop(0, 2)
         def _(k):
             sign = 1 - 2 * k
-            self.copy(stage, k, sign).wait_recv()
+            self.copy(stage, k, k, sign).wait_recv()
             mine = self.source(stage, k, (m + 4 + sign) % 4)
-            send[4 + k] = (mine + recv[k].astype(F32)).astype(SENT[stage])
-            self.copy(stage, 4 + k, sign).start()
+            slot = 3 + 2 * k
+            total = mine + recv[k].astype(F32)
+            self.sender(stage, slot)[...] = total.astype(SENT[stage])
+            self.copy(stage, slot, 2 + k, sign).start()
 
     def third(self, stage):
         m = self.where[ORDERS[self.p][stage]]
@@ -113,15 +122,12 @@
         @pl.loop(0, 2)
         def _(h):
             mine = self.source(stage, h, m)
-            self.copy(stage, 3 - h, 1).wait_recv()
-            self.copy(stage, 4 + h, 1).wait_recv()
-            total = mine + recv[3 - h].astype(F32) + recv[4 + h].astype(F32)
+            self.copy(stage, pl.ds(2 + 2 * h, 2), 2 + h, 1).wait_recv()
+            total = mine + recv[2 + 2 * h].astype(F32) + recv[3 + 2 * h].astype(F32)
             self.place(stage, h, total)
 
     def drain(self, stage):
-        @pl.loop(0, 6)
-        def _(slot):
-            self.copy(stage, slot, 1).wait_send()
+        self.copy(stage, pl.ds(0, 6), 0, 1).wait_send()
 
 
 class Small:
@@ -172,7 +178,7 @@
     barrier = pltpu.get_barrier_semaphore()
     for to in others(where):
         pl.semaphore_signal(barrier, inc=1, device_id=to, device_id_type=MESH)
-    pl.semaphore_wait(barrier, 12)
+    return barrier
 
 
 def partner():
@@ -186,9 +192,6 @@
 def others(where):
     near = [peer(where, dim, shift) for dim in "zyx" for shift in (1, 2, 3)]
     return near + [along(-1), along(1), partner()]
-
-
-AGAIN = {(2, 0): (0, 0), (2, 1): (0, 2), (2, 2): (0, 1)}
 
 
 def part_scratch():
@@ -198,29 +201,25 @@
             for stage in range(3):
                 shape = pltpu.VMEM((6, ROWS[stage], width), SENT[stage])
                 shapes.append(shape)
-                if (r, p) not in AGAIN:
+                if (r, stage) != (2, 0):
                     shapes.append(shape)
                 if stage < 2:
                     shapes.append(pltpu.VMEM((ROWS[stage] // 32, 64, width), F32))
-            shapes.append(pltpu.SemaphoreType.DMA((18,)))
-            shapes.append(pltpu.SemaphoreType.DMA((18,)))
+            shapes.append(pltpu.SemaphoreType.DMA((3,)))
+            shapes.append(pltpu.SemaphoreType.DMA((12,)))
     return shapes
 
 
-def take_parts(where, r, lhs_t, rhs, out, pool, earlier):
+def take_parts(where, r, lhs_t, rhs, out, pool, spare=None):
     parts, off = [], 0
     for p, width in enumerate(WIDTHS[r]):
         bufs = []
         for stage in range(3):
             recv = next(pool)
-            if (r, p) in AGAIN:
-                r0, p0 = AGAIN[(r, p)]
-                send = earlier[r0][p0].bufs[stage][0]
-            else:
-                send = next(pool)
+            send = None if (r, stage) == (2, 0) else next(pool)
             bufs.append((send, recv, next(pool) if stage < 2 else None))
         sems = (next(pool), next(pool))
-        parts.append(Part(where, p, lhs_t, rhs, (off, width), out, bufs, sems))
+        parts.append(Part(where, p, lhs_t, rhs, (off, width), out, bufs, sems, spare))
         off += width
     return parts
 
@@ -242,20 +241,20 @@
 
 def whole_kernel(
     feat_hbm, wv_hbm, wg_hbm, wo_hbm, taps_in, gain_in, cot_hbm,
-    vgrad_hbm, ggrad_hbm, value_out, gate_out, out_out, small_out,
-    feat, cot, feat_t, cot_t, wbuf, wobuf, acc0, acc1, acc2, vhalf, ghalf,
+    vgrad_hbm, ggrad_hbm, vw_hbm, gw_hbm, ow_hbm, small_hbm,
+    value_out, gate_out, out_out, small_out, feat, cot, feat_t, cot_t, wbuf, wobuf, acc0, acc1, acc2, vhalf, ghalf,
     ext, gext, taps, gains, act, vlow, glow, edges, edges_in, gedges, gedges_in,
     stats, stats_in, inv_rows, cols, slots, sums,
     w_sem, wo_sem, f_sem, f_ssem, f_rsem, c_sem, c_ssem, c_rsem,
-    e_ssem, e_rsem, s_ssem, s_rsem, o_sem, small_ssem, small_rsem, *pool,
+    e_ssem, e_rsem, s_ssem, s_rsem, o_sem, r_sem, small_ssem, small_rsem, *pool,
 ):
     where = coords()
     sp, tp = lax.axis_index("sp"), lax.axis_index("tp")
     pool = iter(pool)
     tiny = Small(where, cols, slots, sums, small_out, (small_ssem, small_rsem))
-    out_parts = take_parts(where, 0, cot_t, act, out_out, pool, ())
-    value_parts = take_parts(where, 1, feat_t, vlow, value_out, pool, ())
-    gate_parts = take_parts(where, 2, feat_t, glow, gate_out, pool, (out_parts,))
+    out_parts = take_parts(where, 0, cot_t, act, out_out, pool)
+    value_parts = take_parts(where, 1, feat_t, vlow, value_out, pool)
+    gate_parts = take_parts(where, 2, feat_t, glow, gate_out, pool, cot)
 
     def run(name, parts, stage):
         for part in parts:
@@ -288,19 +287,15 @@
             src.at[:, cut(k)], dst.at[tp, :, cut(k)], ssem.at[k], rsem.at[k], partner()
         )
 
+    barrier = greet(where)
     for k in range(2):
-        own(feat_hbm, feat, f_sem, k).start()
         for c in w_loads(k):
             c.start()
-    greet(where)
-    for k in range(4):
-        give(feat_hbm, feat, f_ssem, f_rsem, k).start()
-    for k in range(2, 4):
         own(feat_hbm, feat, f_sem, k).start()
     for c in w_loads(2):
         c.start()
-    for k in range(4):
-        give(cot_hbm, cot, c_ssem, c_rsem, k).start()
+    for k in range(2, 4):
+        own(feat_hbm, feat, f_sem, k).start()
     for k in range(4):
         own(cot_hbm, cot, c_sem, k).start()
     for k in range(3):
@@ -319,12 +314,12 @@
             acc[2 * c] += got[:, :128]
             acc[2 * c + 1] += got[:, 128:]
 
-    def project(lo, arrived):
-        @pl.loop(lo, lo + 4)
+    def project(lo, hi, arrived):
+        @pl.loop(lo, hi)
         def _(k):
             for c in w_loads(k):
                 c.wait()
-            arrived(k - lo)
+            arrived(k % 4)
             x = feat[half_of(k), :, cut(k % 4)]
             for i, acc in enumerate((acc0, acc1)):
                 add_dot(acc, x, wbuf[k % 3, i])
@@ -334,8 +329,28 @@
                 for c in w_loads(k + 3):
                     c.start()
 
-    project(0, lambda k: own(feat_hbm, feat, f_sem, k).wait())
-    project(4, lambda k: give(feat_hbm, feat, f_ssem, f_rsem, k).wait_recv())
+    def cot_step(lo, hi, arrived):
+        @pl.loop(lo, hi)
+        def _(k):
+            wo_load(k).wait()
+            arrived(k % 4)
+            h = half_of(k)
+            add_dot(acc2, cot[h, :, cut(k % 4)], wobuf[k % 3])
+            flip(cot, cot_t, h, k % 4)
+
+            @pl.when(k + 3 < 8)
+            def _():
+                wo_load(k + 3).start()
+
+    project(0, 2, lambda k: own(feat_hbm, feat, f_sem, k).wait())
+    pl.semaphore_wait(barrier, 12)
+    for k in range(4):
+        give(feat_hbm, feat, f_ssem, f_rsem, k).start()
+    for k in range(4):
+        give(cot_hbm, cot, c_ssem, c_rsem, k).start()
+    project(2, 4, lambda k: own(feat_hbm, feat, f_sem, k).wait())
+    cot_step(0, 4, lambda k: own(cot_hbm, cot, c_sem, k).wait())
+    project(4, 8, lambda k: give(feat_hbm, feat, f_ssem, f_rsem, k).wait_recv())
 
     def gate_rows(at):
         kept = []
@@ -364,21 +379,7 @@
     def _(b):
         gate_rows(pl.multiple_of(b * 32, 32))
 
-    def cot_step(lo, arrived):
-        @pl.loop(lo, lo + 4)
-        def _(k):
-            wo_load(k).wait()
-            arrived(k - lo)
-            h = half_of(k)
-            add_dot(acc2, cot[h, :, cut(k % 4)], wobuf[k % 3])
-            flip(cot, cot_t, h, k % 4)
-
-            @pl.when(k + 3 < 8)
-            def _():
-                wo_load(k + 3).start()
-
-    cot_step(0, lambda k: own(cot_hbm, cot, c_sem, k).wait())
-    cot_step(4, lambda k: give(cot_hbm, cot, c_ssem, c_rsem, k).wait_recv())
+    cot_step(4, 8, lambda k: give(cot_hbm, cot, c_ssem, c_rsem, k).wait_recv())
 
     def fill(buf, got, i):
         inside = sp > 0 if i == 0 else sp < 63
@@ -455,7 +456,10 @@
     share(1).start()
     for c in range(4):
         cols[c, 31:32] = jnp.sum(gain_sums[c], axis=0, keepdims=True)
-    run("first", out_parts, 0)
+    @pl.loop(0, 4)
+    def _(k):
+        flip(feat, feat_t, 1 - tp, k)
+
     share(1).wait_recv()
 
     def conv_grad(at):
@@ -475,30 +479,11 @@
     for i in range(2):
         edge(gedges, gedges_in, i, 2).start()
 
+    run("first", out_parts, 0)
+
     @pl.loop(1, 15)
     def _(b):
         conv_grad(pl.multiple_of(b * 32, 32))
-
-    run("second", out_parts, 0)
-
-    @pl.loop(0, 4)
-    def _(c):
-        @pl.loop(0, 64, init_carry=(none,) * 31)
-        def tap_sums(b, carry):
-            at = pl.multiple_of(b * 8, 8)
-            grad = gext[c, pl.ds(at + 16, 8)]
-            return tuple(
-                carry[k] + grad * ext[c, pl.ds(at + (k + 1), 8)] for k in range(31)
-            )
-
-        for k in range(31):
-            cols[c, k : k + 1] = jnp.sum(tap_sums[k], axis=0, keepdims=True)
-
-    tiny.send(0)
-
-    @pl.loop(0, 4)
-    def _(k):
-        flip(feat, feat_t, 1 - tp, k)
 
     for i in range(2):
         edge(gedges, gedges_in, 1 - i, 2).wait_recv()
@@ -528,51 +513,70 @@
             src.at[c], dst.at[:, 128 * c : 128 * c + 128], o_sem.at[i, c]
         )
 
+    def leave(i):
+        src = (value_out, gate_out, out_out, small_out)[i]
+        dst = (vw_hbm, gw_hbm, ow_hbm, small_hbm)[i]
+        return pltpu.make_async_copy(src, dst, r_sem.at[i])
+
     for i in range(2):
         for c in range(4):
             store(i, c).start()
 
     run("first", value_parts, 0)
-    for part in out_parts:
-        part.drain(0)
+    run("second", out_parts, 0)
     run("first", gate_parts, 0)
     run("third", out_parts, 0)
     run("first", out_parts, 1)
-    tiny.collect(0)
-    tiny.send(1)
+    @pl.loop(0, 4)
+    def _(c):
+        @pl.loop(0, 16, init_carry=(none,) * 31)
+        def tap_sums(b, carry):
+            at = pl.multiple_of(b * 32, 32)
+            grad = gext[c, pl.ds(at + 16, 32)]
+            return tuple(
+                carry[k] + fold(grad * ext[c, pl.ds(at + (k + 1), 32)]) for k in range(31)
+            )
+
+        for k in range(31):
+            cols[c, k : k + 1] = jnp.sum(tap_sums[k], axis=0, keepdims=True)
+
+    tiny.send(0)
+
     run("second", value_parts, 0)
     run("second", gate_parts, 0)
     run("second", out_parts, 1)
-    tiny.collect(1)
-    tiny.send(2)
     run("third", value_parts, 0)
     run("first", value_parts, 1)
+    tiny.collect(0)
+    tiny.send(1)
     run("third", out_parts, 1)
     run("first", out_parts, 2)
-    tiny.collect(2)
-    tiny.send(3)
-    for part in out_parts:
-        part.drain(1)
     run("third", gate_parts, 0)
     run("first", gate_parts, 1)
     run("second", value_parts, 1)
+    tiny.collect(1)
+    tiny.send(2)
     run("second", out_parts, 2)
     run("second", gate_parts, 1)
-    run("third", out_parts, 2)
-    for part in out_parts:
-        part.drain(2)
     run("third", value_parts, 1)
     run("first", value_parts, 2)
+    tiny.collect(2)
+    tiny.send(3)
     run("third", gate_parts, 1)
     run("first", gate_parts, 2)
+    run("third", out_parts, 2)
+    leave(2).start()
     run("second", value_parts, 2)
     run("second", gate_parts, 2)
+    run("third", value_parts, 2)
+    leave(0).start()
+    run("third", gate_parts, 2)
+    leave(1).start()
     tiny.collect(3)
-    run("third", value_parts, 2)
-    run("third", gate_parts, 2)
+    leave(3).start()
 
     tiny.drain()
-    for part in (*value_parts, *gate_parts):
+    for part in (*out_parts, *value_parts, *gate_parts):
         for stage in range(3):
             part.drain(stage)
     for k in range(4):
@@ -584,6 +588,37 @@
         share(i).wait_send()
         for c in range(4):
             store(i, c).wait()
+    for i in range(4):
+        leave(i).wait()
+
+
+def hand_kernel(vgrad, ggrad, vw, gw, ow, small, vgrad_o, ggrad_o, vw_o, gw_o, ow_o,
+                taps_o, gain_o, big, mid, tiny, taps, gain, in_sem, out_sem):
+    moves = []
+    for i, (src, dst) in enumerate(((vgrad, vgrad_o), (ggrad, ggrad_o))):
+        for q in range(4):
+            rows = pl.ds(q * 128, 128)
+            moves.append((src.at[rows], big.at[i, rows], [(big.at[i, rows], dst.at[rows])]))
+    for i, (src, dst) in enumerate(((vw, vw_o), (gw, gw_o), (ow, ow_o))):
+        moves.append((src, mid.at[i], [(mid.at[i], dst)]))
+    moves.append((small, tiny, [(taps, taps_o), (gain, gain_o)]))
+    ins = [
+        pltpu.make_async_copy(src, held, in_sem.at[i]) for i, (src, held, _) in enumerate(moves)
+    ]
+    outs, at = [], 0
+    for copy in ins:
+        copy.start()
+    for copy, (_, _, goes) in zip(ins, moves):
+        copy.wait()
+        if len(goes) == 2:
+            taps[...] = tiny[0:31]
+            gain[...] = tiny[31:32]
+        for src, dst in goes:
+            outs.append(pltpu.make_async_copy(src, dst, out_sem.at[at]))
+            outs[-1].start()
+            at += 1
+    for copy in outs:
+        copy.wait()
 
 
 def on_device(features, weight_value, weight_gate, weight_out, conv_taps, norm_gain, out_grad):
@@ -597,8 +632,10 @@
         whole_kernel,
         out_shape=(grad, grad, piece, piece, piece, jax.ShapeDtypeStruct((32, 512), F32)),
         in_specs=[hbm, hbm, hbm, hbm, vmem, vmem, hbm],
-        out_specs=(hbm, hbm, vmem, vmem, vmem, vmem),
+        out_specs=(hbm,) * 6,
         scratch_shapes=[
+            *[pltpu.VMEM((64, 512), F32)] * 3,
+            pltpu.VMEM((32, 512), F32),
             pltpu.VMEM((2, 512, 2048), BF16),
             pltpu.VMEM((2, 512, 2048), BF16),
             pltpu.VMEM((4, 4, 4, 64, 512), BF16),
@@ -630,7 +667,7 @@
             dma((3, 2)), dma((3,)),
             dma((4,)), dma((4,)), dma((4,)),
             dma((4,)), dma((4,)), dma((4,)),
-            dma((4,)), dma((4,)), dma((2,)), dma((2,)), dma((2, 4)),
+            dma((4,)), dma((4,)), dma((2,)), dma((2,)), dma((2, 4)), dma((4,)),
             dma((16,)), dma((16,)),
             *part_scratch(),
         ],
@@ -638,7 +675,24 @@
             collective_id=0, has_side_effects=True, vmem_limit_bytes=64 * 1024 * 1024 - 65536
         ),
     )(features, weight_value, weight_gate, weight_out, conv_taps, norm_gain[None], out_grad)
-    return vgrad, ggrad, vw, gw, ow, small[:31], small[31]
+    *rest, gain = pl.pallas_call(
+        hand_kernel,
+        out_shape=(
+            grad, grad, piece, piece, piece,
+            jax.ShapeDtypeStruct((31, 512), F32), jax.ShapeDtypeStruct((1, 512), F32),
+        ),
+        in_specs=[hbm] * 6,
+        out_specs=(hbm,) * 7,
+        scratch_shapes=[
+            pltpu.VMEM((2, 512, 512), F32),
+            pltpu.VMEM((3, 64, 512), F32),
+            pltpu.VMEM((32, 512), F32),
+            pltpu.VMEM((31, 512), F32),
+            pltpu.VMEM((1, 512), F32),
+            dma((12,)), dma((13,)),
+        ],
+    )(vgrad, ggrad, vw, gw, ow, small)
+    return (*rest, gain[0])
 
 
 def solution(mesh):

time: 117 us -> 100 us (0.85)
  local copies, waits for them, and re-layouts: 8.5 us -> 0 us
  Pallas kernels: 107 us -> 99.2 us
    pallas_call x1, Pallas kernels: 107 us -> 96.5 us  [on_device(): pl.pallas_call(whole_kernel, out_shape=(grad, grad, piece, piece, piece,...]
    unnamed x14 -> x0, local copies, waits for them, and re-layouts: 7.14 us -> none
    pallas_call x0 -> x1, Pallas kernels: none -> 2.62 us  [on_device(): pl.pallas_call(hand_kernel, out_shape=(grad, grad, piece, piece, piece, j...]
    slice x1 -> x0, local copies, waits for them, and re-layouts: 1.36 us -> none  [on_device(): return (vgrad, ggrad, vw, gw, ow, small[:31], small[31])]
where the time goes in v4:
time: 100 us; the launch traced here: 99.8 us
  Pallas kernels  99.2 us (99%)
    pallas_call x1, Pallas kernels, on_device(): pl.pallas_call(whole_kernel, out_shape=(grad, grad, piece, piece, piece,...  96.5 us
    pallas_call x1, Pallas kernels, on_device(): pl.pallas_call(hand_kernel, out_shape=(grad, grad, piece, piece, piece, j...  2.62 us

profile of v4, /device:TPU:0, one launch (start us, length us, event | category | flops | bytes accessed | tf_op | source)
XLA Modules:
  0.0 99.8 jit_solution(11806929117596086074)
XLA Ops:
  0.6 96.5 %shard_map.126 = (f32[512,512]{1,0:T(8,128)}, f32[512,512]{1,0:T(8,128)}, f32[64,512]{1,0:T(8,128)}, f32[64,512]{1,0:T(8,128)}, f32[64,512]{1,0:T(8,128)}, /*index=5*/f32[32,512]{1,0:T(8,128)}) custom-call(bf16[512,2048]{1,0:T(8,128)(2,1)} %feat_hbm.1, bf16[4096,512]{1,0:T(8,128)(2,1)} %wv_hbm.1, bf16[4096,512]{1,0:T(8,128)(2,1)} %wg_hbm.1, ...), custom_call_target="tpu_custom_call" | custom-call | tf_op jit(solution)/shard_map/pallas_call | solution.py:631
  97.2 2.6 %shard_map.127 = (f32[512,512]{1,0:T(8,128)}, f32[512,512]{1,0:T(8,128)}, f32[64,512]{1,0:T(8,128)}, f32[64,512]{1,0:T(8,128)}, f32[64,512]{1,0:T(8,128)}, /*index=5*/f32[31,512]{1,0:T(8,128)}, f32[1,512]{1,0:T(1,128)}) custom-call(f32[512,512]{1,0:T(8,128)} %get-tuple-element.20.vgrad, f32[512,512]{1,0:T(8,128)} %get-tuple-element.21.ggrad, ...), custom_call_target="tpu_custom_call" | custom-call | tf_op jit(solution)/shard_map/pallas_call | solution.py:678

commit v5 on v4

--- a/solution.py
+++ b/solution.py
@@ -387,10 +387,6 @@
             rows = got[1 - i, c].astype(F32)
             buf[c, 528 * i : 528 * i + 16] = jnp.where(inside, rows, 0.0)
 
-    for i in range(2):
-        edge(edges, edges_in, 1 - i, 0).wait_recv()
-        fill(ext, edges_in, i)
-
     def conv(buf, c, at, first, step):
         total = jnp.zeros((64, 128), F32)
         for k in range(31):
@@ -401,8 +397,7 @@
     def share(n):
         return remote(stats.at[n], stats_in.at[n], s_ssem.at[n], s_rsem.at[n], partner())
 
-    @pl.loop(0, 8)
-    def _(b):
+    def conv_rows(b):
         at = pl.multiple_of(b * 64, 64)
         zero = jnp.zeros((64, 128), F32)
 
@@ -415,6 +410,12 @@
         stats[0, 0, pl.ds(at, 64)] = totals[0]
         stats[0, 1, pl.ds(at, 64)] = totals[1]
 
+    pl.loop(1, 7)(conv_rows)
+    for i in range(2):
+        edge(edges, edges_in, 1 - i, 0).wait_recv()
+        fill(ext, edges_in, i)
+
+    pl.loop(0, 8, step=7)(conv_rows)
     share(0).start()
 
     @pl.loop(0, 4)
@@ -456,10 +457,7 @@
     share(1).start()
     for c in range(4):
         cols[c, 31:32] = jnp.sum(gain_sums[c], axis=0, keepdims=True)
-    @pl.loop(0, 4)
-    def _(k):
-        flip(feat, feat_t, 1 - tp, k)
-
+    run("first", out_parts[2:], 0)
     share(1).wait_recv()
 
     def conv_grad(at):
@@ -479,18 +477,13 @@
     for i in range(2):
         edge(gedges, gedges_in, i, 2).start()
 
-    run("first", out_parts, 0)
+    run("first", out_parts[:2], 0)
 
     @pl.loop(1, 15)
     def _(b):
         conv_grad(pl.multiple_of(b * 32, 32))
 
-    for i in range(2):
-        edge(gedges, gedges_in, 1 - i, 2).wait_recv()
-        fill(gext, gedges_in, i)
-
-    @pl.loop(0, 8)
-    def _(b):
+    def grad_rows(b):
         at = pl.multiple_of(b * 64, 64)
         rows = pl.ds(at, 64)
 
@@ -507,6 +500,18 @@
             vlow[rows, lanes] = vgrad.astype(BF16)
             glow[rows, lanes] = ggrad.astype(BF16)
 
+    @pl.loop(0, 4)
+    def _(k):
+        flip(feat, feat_t, 1 - tp, k)
+
+    pl.loop(1, 7)(grad_rows)
+    run("second", out_parts[:2], 0)
+    for i in range(2):
+        edge(gedges, gedges_in, 1 - i, 2).wait_recv()
+        fill(gext, gedges_in, i)
+
+    pl.loop(0, 8, step=7)(grad_rows)
+
     def store(i, c):
         src, dst = ((acc0, vgrad_hbm), (acc1, ggrad_hbm))[i]
         return pltpu.make_async_copy(
@@ -522,11 +527,11 @@
         for c in range(4):
             store(i, c).start()
 
-    run("first", value_parts, 0)
-    run("second", out_parts, 0)
     run("first", gate_parts, 0)
-    run("third", out_parts, 0)
-    run("first", out_parts, 1)
+    run("first", [value_parts[p] for p in (1, 2, 0)], 0)
+    gate_parts[0].second(0)
+    out_parts[2].second(0)
+    gate_parts[2].second(0)
     @pl.loop(0, 4)
     def _(c):
         @pl.loop(0, 16, init_carry=(none,) * 31)
@@ -541,37 +546,75 @@
             cols[c, k : k + 1] = jnp.sum(tap_sums[k], axis=0, keepdims=True)
 
     tiny.send(0)
-
-    run("second", value_parts, 0)
-    run("second", gate_parts, 0)
-    run("second", out_parts, 1)
-    run("third", value_parts, 0)
-    run("first", value_parts, 1)
+    gate_parts[1].second(0)
+    out_parts[0].third(0)
+    out_parts[0].first(1)
+    out_parts[1].third(0)
+    run("second", [value_parts[p] for p in (2, 0)], 0)
+    out_parts[1].first(1)
+    value_parts[1].second(0)
+    out_parts[2].third(0)
     tiny.collect(0)
     tiny.send(1)
-    run("third", out_parts, 1)
-    run("first", out_parts, 2)
-    run("third", gate_parts, 0)
-    run("first", gate_parts, 1)
-    run("second", value_parts, 1)
+    gate_parts[0].third(0)
+    out_parts[2].first(1)
+    gate_parts[0].first(1)
+    gate_parts[2].third(0)
+    gate_parts[2].first(1)
+    out_parts[0].second(1)
+    gate_parts[1].third(0)
+    gate_parts[1].first(1)
+    value_parts[0].third(0)
+    value_parts[0].first(1)
+    run("third", [value_parts[p] for p in (2, 1)], 0)
+    value_parts[1].first(1)
     tiny.collect(1)
     tiny.send(2)
-    run("second", out_parts, 2)
-    run("second", gate_parts, 1)
-    run("third", value_parts, 1)
-    run("first", value_parts, 2)
+    value_parts[2].first(1)
+    run("second", [out_parts[p] for p in (2, 1)], 1)
+    gate_parts[0].second(1)
+    out_parts[0].third(1)
+    out_parts[0].first(2)
+    run("second", [gate_parts[p] for p in (1, 2)], 1)
+    run("second", value_parts, 1)
+    gate_parts[0].third(1)
+    gate_parts[0].first(2)
+    out_parts[1].third(1)
+    out_parts[1].first(2)
+    out_parts[2].third(1)
     tiny.collect(2)
     tiny.send(3)
-    run("third", gate_parts, 1)
-    run("first", gate_parts, 2)
-    run("third", out_parts, 2)
+    out_parts[2].first(2)
+    out_parts[0].second(2)
+    gate_parts[1].third(1)
+    gate_parts[1].first(2)
+    value_parts[0].third(1)
+    value_parts[0].first(2)
+    value_parts[1].third(1)
+    value_parts[1].first(2)
+    gate_parts[2].third(1)
+    gate_parts[2].first(2)
+    value_parts[2].third(1)
+    value_parts[2].first(2)
+    out_parts[1].second(2)
+    gate_parts[0].second(2)
+    out_parts[0].third(2)
+    out_parts[2].second(2)
+    gate_parts[1].second(2)
+    value_parts[0].second(2)
+    gate_parts[2].second(2)
+    run("second", [value_parts[p] for p in (1, 2)], 2)
+    gate_parts[0].third(2)
+    out_parts[1].third(2)
+    out_parts[2].third(2)
     leave(2).start()
-    run("second", value_parts, 2)
-    run("second", gate_parts, 2)
-    run("third", value_parts, 2)
+    gate_parts[1].third(2)
+    gate_parts[2].third(2)
+    leave(1).start()
+    value_parts[0].third(2)
+    value_parts[1].third(2)
+    value_parts[2].third(2)
     leave(0).start()
-    run("third", gate_parts, 2)
-    leave(1).start()
     tiny.collect(3)
     leave(3).start()
 

time: 100 us -> 89.1 us (0.89)
  Pallas kernels: 99.2 us -> 88.2 us
    pallas_call x1, Pallas kernels: 96.5 us -> 85.6 us  [on_device(): pl.pallas_call(whole_kernel, out_shape=(grad, grad, piece, piece, piece,...]
where the time goes in v5:
time: 89.1 us; the launch traced here: 88.8 us
  Pallas kernels  88.2 us (99%)
    pallas_call x1, Pallas kernels, on_device(): pl.pallas_call(whole_kernel, out_shape=(grad, grad, piece, piece, piece,...  85.6 us
    pallas_call x1, Pallas kernels, on_device(): pl.pallas_call(hand_kernel, out_shape=(grad, grad, piece, piece, piece, j...  2.62 us

profile of v5, /device:TPU:0, one launch (start us, length us, event | category | flops | bytes accessed | tf_op | source)
XLA Modules:
  0.0 88.8 jit_solution(12204239580296390883)
XLA Ops:
  0.6 85.6 %shard_map.126 = (f32[512,512]{1,0:T(8,128)}, f32[512,512]{1,0:T(8,128)}, f32[64,512]{1,0:T(8,128)}, f32[64,512]{1,0:T(8,128)}, f32[64,512]{1,0:T(8,128)}, /*index=5*/f32[32,512]{1,0:T(8,128)}) custom-call(bf16[512,2048]{1,0:T(8,128)(2,1)} %feat_hbm.1, bf16[4096,512]{1,0:T(8,128)(2,1)} %wv_hbm.1, bf16[4096,512]{1,0:T(8,128)(2,1)} %wg_hbm.1, ...), custom_call_target="tpu_custom_call" | custom-call | tf_op jit(solution)/shard_map/pallas_call | solution.py:674
  86.2 2.6 %shard_map.127 = (f32[512,512]{1,0:T(8,128)}, f32[512,512]{1,0:T(8,128)}, f32[64,512]{1,0:T(8,128)}, f32[64,512]{1,0:T(8,128)}, f32[64,512]{1,0:T(8,128)}, /*index=5*/f32[31,512]{1,0:T(8,128)}, f32[1,512]{1,0:T(1,128)}) custom-call(f32[512,512]{1,0:T(8,128)} %get-tuple-element.20.vgrad, f32[512,512]{1,0:T(8,128)} %get-tuple-element.21.ggrad, ...), custom_call_target="tpu_custom_call" | custom-call | tf_op jit(solution)/shard_map/pallas_call | solution.py:721

commit v6 on v5

--- a/solution.py
+++ b/solution.py
@@ -17,7 +17,7 @@
 WIDTHS = ((128, 128, 256), (256, 128, 128), (128, 256, 128))
 ORDERS = ("xzy", "yxz", "zyx")
 ROWS = (512, 128, 32)
-SENT = (BF16, BF16, F32)
+SENT = (BF16, BF16, BF16)
 
 
 def coords():
@@ -60,14 +60,10 @@
                 at = (j // 2) * 8 + j % 2
                 two = [held[at + 2 * (2 * h + i)] for i in range(2)]
                 return jnp.concatenate(two, axis=0)
-            return held[pl.ds(4 * j + 2 * h, 2)].reshape(128, width)
-        return held[j, pl.ds(pl.multiple_of(h * 32, 32), 32)]
+        return held[pl.ds(4 * j + 2 * h, 2)].reshape(128, width)
 
     def place(self, stage, h, value):
-        off, width = self.cols
-        if stage == 2:
-            self.out[pl.ds(pl.multiple_of(h * 32, 32), 32), off : off + width] = value
-            return
+        width = self.cols[1]
         held = self.bufs[stage][2]
         count = ROWS[stage] // 64
         held[pl.ds(count * h, count)] = value.reshape(count, 64, width)
@@ -89,8 +85,20 @@
             peer(self.where, ORDERS[self.p][stage], sign),
         )
 
+    def straight(self, k):
+        send, recv, _ = self.bufs[2]
+        ssem, rsem = self.sems
+        return remote(send.at[k], recv.at[k], ssem.at[2], rsem.at[8 + k],
+                      peer(self.where, ORDERS[self.p][2], k + 1))
+
     def first(self, stage):
         m = self.where[ORDERS[self.p][stage]]
+        if stage == 2:
+            for k in (1, 0, 2):
+                self.bufs[2][0][k] = self.bufs[1][2][(m + k + 1) % 4].astype(BF16)
+            for k in (1, 0, 2):
+                self.straight(k).start()
+            return
 
         @pl.loop(0, 4)
         def _(i):
@@ -118,6 +126,14 @@
     def third(self, stage):
         m = self.where[ORDERS[self.p][stage]]
         recv = self.bufs[stage][1]
+        if stage == 2:
+            total = self.bufs[1][2][m]
+            for k in range(3):
+                self.straight(k).wait_recv()
+                total = total + recv[k].astype(F32)
+            off, width = self.cols
+            self.out[:, off : off + width] = total
+            return
 
         @pl.loop(0, 2)
         def _(h):
@@ -127,7 +143,177 @@
             self.place(stage, h, total)
 
     def drain(self, stage):
+        if stage == 2:
+            recv = self.bufs[2][1]
+            ssem, rsem = self.sems
+            to = peer(self.where, ORDERS[self.p][2], 1)
+            remote(recv, recv, ssem.at[2], rsem.at[8], to).wait_send()
+            return
         self.copy(stage, pl.ds(0, 6), 0, 1).wait_send()
+
+
+class Gathered(Part):
+    def own_rows(self, h):
+        m = self.where[ORDERS[self.p][0]]
+        return ring_piece(self.lhs_t, self.p, m, h)[...].reshape(512, 512)
+
+    def ring(self, src, dst, sem, sign):
+        ssem, rsem = self.sems
+        return remote(src, dst, ssem.at[0], rsem.at[sem],
+                      peer(self.where, ORDERS[self.p][0], sign))
+
+    def first(self, stage):
+        if stage:
+            return Part.first(self, stage)
+        off, width = self.cols
+        recv, mine = self.bufs[0][1], self.rhs.at[:, off : off + width]
+        self.ring(mine, recv.at[0], 0, 1).start()
+        self.ring(mine, recv.at[1], 1, -1).start()
+
+    def second(self, stage):
+        if stage:
+            return Part.second(self, stage)
+        recv = self.bufs[0][1]
+        for k, sign in enumerate((1, -1)):
+            self.ring(recv.at[k], recv.at[k], k, sign).wait_recv()
+            rows = pl.ds(256 * k, 256)
+            self.ring(recv.at[k, rows], recv.at[2, rows], 2, sign).start()
+
+    def middle(self, stage):
+        off, width = self.cols
+        recv, held = self.bufs[0][1:]
+
+        @pl.loop(0, 2)
+        def _(h):
+            got = jnp.dot(self.own_rows(h), self.rhs[:, off : off + width],
+                          preferred_element_type=F32)
+            for slot in range(2):
+                rows = self.lhs[slot, h].reshape(512, 512)
+                got = got + jnp.dot(rows, recv[slot], preferred_element_type=F32)
+            held[pl.ds(8 * h, 8)] = got.reshape(8, 64, width)
+
+    def third(self, stage):
+        if stage:
+            return Part.third(self, stage)
+        width = self.cols[1]
+        recv, held = self.bufs[0][1:]
+        self.ring(recv.at[2], recv.at[2], 2, 1).wait_recv()
+
+        @pl.loop(0, 2)
+        def _(h):
+            rows = self.lhs[2, h].reshape(512, 512)
+            got = jnp.dot(rows, recv[2], preferred_element_type=F32)
+            held[pl.ds(8 * h, 8)] += got.reshape(8, 64, width)
+
+    def source(self, stage, h, j):
+        if stage == 1 and self.p == 1:
+            held = self.bufs[0][2]
+            two = [held[(2 * h + i) * 4 + j] for i in range(2)]
+            return jnp.concatenate(two, axis=0)
+        return Part.source(self, stage, h, j)
+
+    def drain(self, stage):
+        if stage:
+            return Part.drain(self, stage)
+        recv = self.bufs[0][1]
+        self.ring(recv, recv, 0, 1).wait_send()
+
+
+def ring_piece(rows_t, p, j, h):
+    if p == 0:
+        return rows_t.at[pl.ds(2 * h, 2), :, j]
+    if p == 1:
+        return rows_t.at[pl.ds(2 * h, 2), j]
+    return rows_t.at[j, pl.ds(2 * h, 2)]
+
+
+class Early:
+    def __init__(self, where, p, rows_t, lhs, relay, sems):
+        self.where, self.p, self.rows_t = where, p, rows_t
+        self.lhs, self.relay = lhs, relay
+        self.rsem, self.ysem, self.dsem, self.ssem, self.d_ssem = sems
+        self.m, self.tp = where[ORDERS[p][0]], lax.axis_index("tp")
+
+    def go(self, src, dst, ssem, rsem, sign):
+        return remote(src, dst, self.ssem.at[ssem], rsem,
+                      peer(self.where, ORDERS[self.p][0], sign))
+
+    def when(self, shift, act):
+        if self.p < 2:
+            act()
+        else:
+            pl.when((self.m + 4 + shift) % 4 // 2 == self.tp)(act)
+
+    def far_copies(self):
+        j = (self.m + 2) % 4
+        for k, sign in enumerate((1, -1)):
+            if self.p < 2:
+                src = ring_piece(self.rows_t, self.p, j, self.tp).at[k]
+            else:
+                src = ring_piece(self.rows_t, self.p, j, k)
+            yield self.go(src, self.relay.at[k], 0, self.ysem.at[k], sign)
+
+    def far(self):
+        self.when(2, lambda: [c.start() for c in self.far_copies()] and None)
+
+    def near_copies(self, k, q):
+        sign = 1 - 2 * k
+        j = (self.m + 4 + sign) % 4
+        if self.p < 2:
+            src = ring_piece(self.rows_t, self.p, j, self.tp).at[q]
+            dst = self.lhs.at[k, self.tp, q]
+        else:
+            src, dst = ring_piece(self.rows_t, self.p, j, q), self.lhs.at[k, q]
+        return self.go(src, dst, 1 + k, self.rsem.at[k], sign)
+
+    def near(self, q):
+        for k in range(2):
+            self.when(1 - 2 * k, lambda: self.near_copies(k, q).start())
+
+    def relays(self, k):
+        dst = self.lhs.at[2, self.tp, k] if self.p < 2 else self.lhs.at[2, k]
+        return self.go(self.relay.at[k], dst, 3 + k, self.rsem.at[2], 1 - 2 * k)
+
+    def pass_on(self):
+        def act(k):
+            sign = 1 - 2 * k
+            self.go(self.relay.at[k], self.relay.at[k], 0, self.ysem.at[k], sign).wait_recv()
+            self.relays(k).start()
+
+        for k in range(2):
+            self.when(1 - 2 * k, lambda: act(k))
+
+    def held(self, slot, half):
+        return self.lhs.at[slot, half] if self.p < 2 else self.lhs.at[slot]
+
+    def across(self, slot, half):
+        ref = self.held(slot, half)
+        return remote(ref, ref, self.d_ssem.at[slot], self.dsem.at[slot], partner())
+
+    def share(self, slot):
+        def act():
+            ref = self.held(slot, self.tp)
+            self.go(ref, ref, 0, self.rsem.at[slot], 1).wait_recv()
+            self.across(slot, self.tp).start()
+
+        self.when(0, act)
+
+    def have(self, slot):
+        wait = lambda: self.across(slot, 1 - self.tp).wait_recv()
+        if self.p < 2:
+            wait()
+        else:
+            pl.when(self.m // 2 != self.tp)(wait)
+
+    def drain(self):
+        two = lambda ref, sem: self.go(ref, ref, sem, self.rsem.at[0], 1).wait_send()
+        self.when(2, lambda: two(self.relay, 0))
+        for k in range(2):
+            piece = self.lhs.at[k, 0] if self.p < 2 else self.lhs.at[k]
+            self.when(1 - 2 * k, lambda: two(piece, 1 + k))
+            self.when(1 - 2 * k, lambda: two(self.relay.at[k], 3 + k))
+        for slot in range(3):
+            self.when(0, lambda: self.across(slot, self.tp).wait_send())
 
 
 class Small:
@@ -197,11 +383,13 @@
 def part_scratch():
     shapes = []
     for r, widths in enumerate(WIDTHS):
-        for p, width in enumerate(widths):
+        for width in widths:
             for stage in range(3):
-                shape = pltpu.VMEM((6, ROWS[stage], width), SENT[stage])
-                shapes.append(shape)
-                if (r, stage) != (2, 0):
+                if stage == 0:
+                    shapes.append(pltpu.VMEM((3 if r else 6, 512, width), BF16))
+                else:
+                    shape = pltpu.VMEM((6, 128, width) if stage == 1 else (3, 64, width), BF16)
+                    shapes.append(shape)
                     shapes.append(shape)
                 if stage < 2:
                     shapes.append(pltpu.VMEM((ROWS[stage] // 32, 64, width), F32))
@@ -210,18 +398,31 @@
     return shapes
 
 
-def take_parts(where, r, lhs_t, rhs, out, pool, spare=None):
+def take_parts(where, r, lhs_t, rhs, out, pool, spare=None, lhs=(None,) * 3):
     parts, off = [], 0
     for p, width in enumerate(WIDTHS[r]):
         bufs = []
         for stage in range(3):
             recv = next(pool)
-            send = None if (r, stage) == (2, 0) else next(pool)
+            send = None if stage == 0 else next(pool)
             bufs.append((send, recv, next(pool) if stage < 2 else None))
         sems = (next(pool), next(pool))
-        parts.append(Part(where, p, lhs_t, rhs, (off, width), out, bufs, sems, spare))
+        kind = Gathered if r else Part
+        part = kind(where, p, lhs_t, rhs, (off, width), out, bufs, sems, spare)
+        part.lhs = lhs[p]
+        parts.append(part)
         off += width
     return parts
+
+
+def early_scratch():
+    dma = pltpu.SemaphoreType.DMA
+    shapes = []
+    for p in range(3):
+        shapes.append(pltpu.VMEM((3, 2, 2, 4, 64, 512), BF16))
+        shapes.append(pltpu.VMEM((2, 4, 64, 512) if p < 2 else (2, 2, 4, 64, 512), BF16))
+        shapes += [dma((3,)), dma((2,)), dma((3,)), dma((5,)), dma((3,))]
+    return shapes
 
 
 def flip(src, dst, h, k):
@@ -252,9 +453,27 @@
     sp, tp = lax.axis_index("sp"), lax.axis_index("tp")
     pool = iter(pool)
     tiny = Small(where, cols, slots, sums, small_out, (small_ssem, small_rsem))
-    out_parts = take_parts(where, 0, cot_t, act, out_out, pool)
-    value_parts = take_parts(where, 1, feat_t, vlow, value_out, pool)
-    gate_parts = take_parts(where, 2, feat_t, glow, gate_out, pool, cot)
+    early = []
+    for p in range(3):
+        lhs, relay = next(pool), next(pool)
+        early.append(Early(where, p, feat_t, lhs, relay, [next(pool) for _ in range(5)]))
+    lhs = [e.lhs for e in early]
+    out_parts = take_parts(where, 0, cot_t, act, out_out, pool, cot)
+    value_parts = take_parts(where, 1, feat_t, vlow, value_out, pool, None, lhs)
+    gate_parts = take_parts(where, 2, feat_t, glow, gate_out, pool, None, lhs)
+
+    def start_round(parts):
+        @pl.loop(0, 4)
+        def _(i):
+            sign = 1 - 2 * (i % 2)
+            h = ((i + 1) // 2) % 2
+            slot = i + (i // 2) * (2 - 3 * (i % 2))
+            for part in parts:
+                m = where[ORDERS[part.p][0]]
+                j = (m + 6 - (i // 2) * sign) % 4
+                part.sender(0, slot)[...] = part.source(0, h, j).astype(BF16)
+            for part in parts:
+                part.copy(0, slot, i + (i // 2) * sign, sign).start()
 
     def run(name, parts, stage):
         for part in parts:
@@ -288,14 +507,11 @@
         )
 
     barrier = greet(where)
-    for k in range(2):
+    for k in range(4):
+        own(feat_hbm, feat, f_sem, k).start()
+    for k in range(3):
         for c in w_loads(k):
             c.start()
-        own(feat_hbm, feat, f_sem, k).start()
-    for c in w_loads(2):
-        c.start()
-    for k in range(2, 4):
-        own(feat_hbm, feat, f_sem, k).start()
     for k in range(4):
         own(cot_hbm, cot, c_sem, k).start()
     for k in range(3):
@@ -342,13 +558,22 @@
             def _():
                 wo_load(k + 3).start()
 
-    project(0, 2, lambda k: own(feat_hbm, feat, f_sem, k).wait())
+    @pl.loop(0, 4)
+    def _(k):
+        own(feat_hbm, feat, f_sem, k).wait()
+        flip(feat, feat_t, tp, k)
+
     pl.semaphore_wait(barrier, 12)
     for k in range(4):
         give(feat_hbm, feat, f_ssem, f_rsem, k).start()
+    for e in early:
+        e.far()
     for k in range(4):
         give(cot_hbm, cot, c_ssem, c_rsem, k).start()
-    project(2, 4, lambda k: own(feat_hbm, feat, f_sem, k).wait())
+    for q in range(2):
+        for e in early[1:]:
+            e.near(q)
+    project(0, 4, lambda k: None)
     cot_step(0, 4, lambda k: own(cot_hbm, cot, c_sem, k).wait())
     project(4, 8, lambda k: give(feat_hbm, feat, f_ssem, f_rsem, k).wait_recv())
 
@@ -374,6 +599,8 @@
             edges[i, c] = kept[c][16 * i : 16 * i + 16]
     for i in range(2):
         edge(edges, edges_in, i, 0).start()
+    for q in range(2):
+        early[0].near(q)
 
     @pl.loop(1, 15)
     def _(b):
@@ -420,7 +647,7 @@
 
     @pl.loop(0, 4)
     def _(k):
-        flip(feat, feat_t, tp, k)
+        flip(feat, feat_t, 1 - tp, k)
 
     share(0).wait_recv()
 
@@ -477,7 +704,7 @@
     for i in range(2):
         edge(gedges, gedges_in, i, 2).start()
 
-    run("first", out_parts[:2], 0)
+    start_round(out_parts[:2])
 
     @pl.loop(1, 15)
     def _(b):
@@ -500,12 +727,10 @@
             vlow[rows, lanes] = vgrad.astype(BF16)
             glow[rows, lanes] = ggrad.astype(BF16)
 
-    @pl.loop(0, 4)
-    def _(k):
-        flip(feat, feat_t, 1 - tp, k)
-
+    for e in early:
+        for slot in range(2):
+            e.share(slot)
     pl.loop(1, 7)(grad_rows)
-    run("second", out_parts[:2], 0)
     for i in range(2):
         edge(gedges, gedges_in, 1 - i, 2).wait_recv()
         fill(gext, gedges_in, i)
@@ -527,11 +752,11 @@
         for c in range(4):
             store(i, c).start()
 
+    run("first", value_parts, 0)
     run("first", gate_parts, 0)
-    run("first", [value_parts[p] for p in (1, 2, 0)], 0)
-    gate_parts[0].second(0)
-    out_parts[2].second(0)
-    gate_parts[2].second(0)
+    for e in early:
+        e.pass_on()
+    value_parts[1].second(0)
     @pl.loop(0, 4)
     def _(c):
         @pl.loop(0, 16, init_carry=(none,) * 31)
@@ -546,79 +771,92 @@
             cols[c, k : k + 1] = jnp.sum(tap_sums[k], axis=0, keepdims=True)
 
     tiny.send(0)
-    gate_parts[1].second(0)
-    out_parts[0].third(0)
-    out_parts[0].first(1)
-    out_parts[1].third(0)
-    run("second", [value_parts[p] for p in (2, 0)], 0)
+
+    run("second", [out_parts[p] for p in (2, 0, 1)], 0)
+    early[1].have(0)
+    early[1].have(1)
+    value_parts[1].middle(0)
+    run("second", [value_parts[p] for p in (0, 2)], 0)
+    early[0].have(0)
+    early[0].have(1)
+    early[2].have(0)
+    early[2].have(1)
+    run("middle", [value_parts[p] for p in (0, 2)], 0)
+    run("second", [gate_parts[p] for p in (0, 1)], 0)
+    gate_parts[0].middle(0)
+    gate_parts[2].second(0)
+    run("middle", [gate_parts[p] for p in (2, 1)], 0)
+    early[0].share(2)
+    early[1].share(2)
+    run("third", [out_parts[p] for p in (0, 1)], 0)
     out_parts[1].first(1)
-    value_parts[1].second(0)
-    out_parts[2].third(0)
     tiny.collect(0)
     tiny.send(1)
+    out_parts[0].first(1)
+    early[1].have(2)
+    early[0].have(2)
+    run("third", [value_parts[p] for p in (1, 0)], 0)
+    early[2].share(2)
+    run("first", [value_parts[p] for p in (0, 1)], 1)
     gate_parts[0].third(0)
+    out_parts[2].third(0)
     out_parts[2].first(1)
+    gate_parts[1].third(0)
     gate_parts[0].first(1)
+    early[2].have(2)
+    value_parts[2].third(0)
+    gate_parts[1].first(1)
+    value_parts[2].first(1)
     gate_parts[2].third(0)
+    out_parts[1].second(1)
+    value_parts[1].second(1)
     gate_parts[2].first(1)
-    out_parts[0].second(1)
-    gate_parts[1].third(0)
-    gate_parts[1].first(1)
-    value_parts[0].third(0)
-    value_parts[0].first(1)
-    run("third", [value_parts[p] for p in (2, 1)], 0)
-    value_parts[1].first(1)
+    run("second", [out_parts[p] for p in (0, 2)], 1)
     tiny.collect(1)
     tiny.send(2)
-    value_parts[2].first(1)
-    run("second", [out_parts[p] for p in (2, 1)], 1)
+    value_parts[0].second(1)
+    gate_parts[1].second(1)
+    value_parts[2].second(1)
     gate_parts[0].second(1)
+    out_parts[1].third(1)
+    out_parts[1].first(2)
+    gate_parts[2].second(1)
     out_parts[0].third(1)
     out_parts[0].first(2)
-    run("second", [gate_parts[p] for p in (1, 2)], 1)
-    run("second", value_parts, 1)
-    gate_parts[0].third(1)
-    gate_parts[0].first(2)
-    out_parts[1].third(1)
-    out_parts[1].first(2)
+    value_parts[1].third(1)
+    value_parts[1].first(2)
+    value_parts[0].third(1)
     out_parts[2].third(1)
     tiny.collect(2)
     tiny.send(3)
     out_parts[2].first(2)
-    out_parts[0].second(2)
+    value_parts[0].first(2)
     gate_parts[1].third(1)
     gate_parts[1].first(2)
-    value_parts[0].third(1)
-    value_parts[0].first(2)
-    value_parts[1].third(1)
-    value_parts[1].first(2)
+    gate_parts[0].third(1)
+    gate_parts[0].first(2)
+    value_parts[2].third(1)
+    value_parts[2].first(2)
     gate_parts[2].third(1)
     gate_parts[2].first(2)
-    value_parts[2].third(1)
-    value_parts[2].first(2)
-    out_parts[1].second(2)
-    gate_parts[0].second(2)
+    out_parts[1].third(2)
     out_parts[0].third(2)
-    out_parts[2].second(2)
-    gate_parts[1].second(2)
-    value_parts[0].second(2)
-    gate_parts[2].second(2)
-    run("second", [value_parts[p] for p in (1, 2)], 2)
-    gate_parts[0].third(2)
-    out_parts[1].third(2)
+    value_parts[1].third(2)
+    value_parts[0].third(2)
     out_parts[2].third(2)
     leave(2).start()
+    value_parts[2].third(2)
+    leave(0).start()
     gate_parts[1].third(2)
+    gate_parts[0].third(2)
     gate_parts[2].third(2)
     leave(1).start()
-    value_parts[0].third(2)
-    value_parts[1].third(2)
-    value_parts[2].third(2)
-    leave(0).start()
     tiny.collect(3)
     leave(3).start()
 
     tiny.drain()
+    for e in early:
+        e.drain()
     for part in (*out_parts, *value_parts, *gate_parts):
         for stage in range(3):
             part.drain(stage)
@@ -712,6 +950,7 @@
             dma((4,)), dma((4,)), dma((4,)),
             dma((4,)), dma((4,)), dma((2,)), dma((2,)), dma((2, 4)), dma((4,)),
             dma((16,)), dma((16,)),
+            *early_scratch(),
             *part_scratch(),
         ],
         compiler_params=pltpu.CompilerParams(

time: 89.1 us -> 83.5 us (0.937)
  Pallas kernels: 88.2 us -> 82.7 us
    pallas_call x1, Pallas kernels: 85.6 us -> 80 us  [on_device(): pl.pallas_call(whole_kernel, out_shape=(grad, grad, piece, piece, piece,...]
where the time goes in v6:
time: 83.5 us; the launch traced here: 83.3 us
  Pallas kernels  82.7 us (99%)
    pallas_call x1, Pallas kernels, on_device(): pl.pallas_call(whole_kernel, out_shape=(grad, grad, piece, piece, piece,...  80 us
    pallas_call x1, Pallas kernels, on_device(): pl.pallas_call(hand_kernel, out_shape=(grad, grad, piece, piece, piece, j...  2.62 us

profile of v6, /device:TPU:0, one launch (start us, length us, event | category | flops | bytes accessed | tf_op | source)
XLA Modules:
  0.0 83.3 jit_solution(3982266059494951791)
XLA Ops:
  0.6 80.0 %shard_map.126 = (f32[512,512]{1,0:T(8,128)}, f32[512,512]{1,0:T(8,128)}, f32[64,512]{1,0:T(8,128)}, f32[64,512]{1,0:T(8,128)}, f32[64,512]{1,0:T(8,128)}, /*index=5*/f32[32,512]{1,0:T(8,128)}) custom-call(bf16[512,2048]{1,0:T(8,128)(2,1)} %feat_hbm.1, bf16[4096,512]{1,0:T(8,128)(2,1)} %wv_hbm.1, bf16[4096,512]{1,0:T(8,128)(2,1)} %wg_hbm.1, ...), custom_call_target="tpu_custom_call" | custom-call | tf_op jit(solution)/shard_map/pallas_call | solution.py:912
  80.7 2.6 %shard_map.127 = (f32[512,512]{1,0:T(8,128)}, f32[512,512]{1,0:T(8,128)}, f32[64,512]{1,0:T(8,128)}, f32[64,512]{1,0:T(8,128)}, f32[64,512]{1,0:T(8,128)}, /*index=5*/f32[31,512]{1,0:T(8,128)}, f32[1,512]{1,0:T(1,128)}) custom-call(f32[512,512]{1,0:T(8,128)} %get-tuple-element.20.vgrad, f32[512,512]{1,0:T(8,128)} %get-tuple-element.21.ggrad, ...), custom_call_target="tpu_custom_call" | custom-call | tf_op jit(solution)/shard_map/pallas_call | solution.py:960

commit v7 on v6

--- a/solution.py
+++ b/solution.py
@@ -14,7 +14,7 @@
 
 NORM_EPS = 1e-05
 
-WIDTHS = ((128, 128, 256), (256, 128, 128), (128, 256, 128))
+WIDTHS = ((128, 256, 128), (128, 128, 256), (256, 128, 128))
 ORDERS = ("xzy", "yxz", "zyx")
 ROWS = (512, 128, 32)
 SENT = (BF16, BF16, BF16)
@@ -684,7 +684,7 @@
     share(1).start()
     for c in range(4):
         cols[c, 31:32] = jnp.sum(gain_sums[c], axis=0, keepdims=True)
-    run("first", out_parts[2:], 0)
+    run("first", out_parts[1:2], 0)
     share(1).wait_recv()
 
     def conv_grad(at):
@@ -704,7 +704,7 @@
     for i in range(2):
         edge(gedges, gedges_in, i, 2).start()
 
-    start_round(out_parts[:2])
+    start_round((out_parts[0], out_parts[2]))
 
     @pl.loop(1, 15)
     def _(b):
@@ -754,9 +754,10 @@
 
     run("first", value_parts, 0)
     run("first", gate_parts, 0)
-    for e in early:
-        e.pass_on()
-    value_parts[1].second(0)
+    early[0].pass_on()
+    early[2].pass_on()
+    early[1].pass_on()
+    run("second", [out_parts[p] for p in (0, 2)], 0)
     @pl.loop(0, 4)
     def _(c):
         @pl.loop(0, 16, init_carry=(none,) * 31)
@@ -772,83 +773,86 @@
 
     tiny.send(0)
 
-    run("second", [out_parts[p] for p in (2, 0, 1)], 0)
+    out_parts[1].second(0)
+    value_parts[0].second(0)
+    early[0].have(0)
+    early[0].have(1)
+    value_parts[0].middle(0)
+    value_parts[2].second(0)
+    early[2].have(0)
+    early[2].have(1)
+    value_parts[2].middle(0)
+    value_parts[1].second(0)
     early[1].have(0)
     early[1].have(1)
     value_parts[1].middle(0)
-    run("second", [value_parts[p] for p in (0, 2)], 0)
-    early[0].have(0)
-    early[0].have(1)
-    early[2].have(0)
-    early[2].have(1)
-    run("middle", [value_parts[p] for p in (0, 2)], 0)
-    run("second", [gate_parts[p] for p in (0, 1)], 0)
+    gate_parts[0].second(0)
     gate_parts[0].middle(0)
-    gate_parts[2].second(0)
+    run("second", [gate_parts[p] for p in (2, 1)], 0)
     run("middle", [gate_parts[p] for p in (2, 1)], 0)
     early[0].share(2)
-    early[1].share(2)
-    run("third", [out_parts[p] for p in (0, 1)], 0)
-    out_parts[1].first(1)
+    out_parts[0].third(0)
     tiny.collect(0)
     tiny.send(1)
+    early[1].share(2)
     out_parts[0].first(1)
-    early[1].have(2)
-    early[0].have(2)
-    run("third", [value_parts[p] for p in (1, 0)], 0)
-    early[2].share(2)
-    run("first", [value_parts[p] for p in (0, 1)], 1)
-    gate_parts[0].third(0)
     out_parts[2].third(0)
     out_parts[2].first(1)
-    gate_parts[1].third(0)
-    gate_parts[0].first(1)
+    early[0].have(2)
+    value_parts[0].third(0)
+    early[2].share(2)
+    value_parts[0].first(1)
+    out_parts[1].third(0)
+    out_parts[1].first(1)
+    gate_parts[0].third(0)
     early[2].have(2)
     value_parts[2].third(0)
+    value_parts[2].first(1)
+    early[1].have(2)
+    value_parts[1].third(0)
+    gate_parts[0].first(1)
+    value_parts[1].first(1)
+    gate_parts[1].third(0)
     gate_parts[1].first(1)
-    value_parts[2].first(1)
     gate_parts[2].third(0)
-    out_parts[1].second(1)
-    value_parts[1].second(1)
+    value_parts[0].second(1)
+    out_parts[0].second(1)
     gate_parts[2].first(1)
-    run("second", [out_parts[p] for p in (0, 2)], 1)
+    run("second", [out_parts[p] for p in (2, 1)], 1)
     tiny.collect(1)
     tiny.send(2)
-    value_parts[0].second(1)
-    gate_parts[1].second(1)
-    value_parts[2].second(1)
-    gate_parts[0].second(1)
+    run("second", [value_parts[p] for p in (2, 1)], 1)
+    run("second", gate_parts, 1)
+    value_parts[0].third(1)
+    out_parts[0].third(1)
+    value_parts[0].first(2)
+    out_parts[0].first(2)
+    out_parts[2].third(1)
+    out_parts[2].first(2)
     out_parts[1].third(1)
     out_parts[1].first(2)
-    gate_parts[2].second(1)
-    out_parts[0].third(1)
-    out_parts[0].first(2)
     value_parts[1].third(1)
     value_parts[1].first(2)
-    value_parts[0].third(1)
-    out_parts[2].third(1)
+    value_parts[2].third(1)
+    value_parts[2].first(2)
+    gate_parts[0].third(1)
+    gate_parts[0].first(2)
+    gate_parts[1].third(1)
+    gate_parts[1].first(2)
+    gate_parts[2].third(1)
+    gate_parts[2].first(2)
+    value_parts[0].third(2)
     tiny.collect(2)
     tiny.send(3)
-    out_parts[2].first(2)
-    value_parts[0].first(2)
-    gate_parts[1].third(1)
-    gate_parts[1].first(2)
-    gate_parts[0].third(1)
-    gate_parts[0].first(2)
-    value_parts[2].third(1)
-    value_parts[2].first(2)
-    gate_parts[2].third(1)
-    gate_parts[2].first(2)
+    out_parts[2].third(2)
+    out_parts[0].third(2)
     out_parts[1].third(2)
-    out_parts[0].third(2)
+    leave(2).start()
     value_parts[1].third(2)
-    value_parts[0].third(2)
-    out_parts[2].third(2)
-    leave(2).start()
     value_parts[2].third(2)
     leave(0).start()
+    gate_parts[0].third(2)
     gate_parts[1].third(2)
-    gate_parts[0].third(2)
     gate_parts[2].third(2)
     leave(1).start()
     tiny.collect(3)

time: 83.5 us -> 83.6 us (level)
  no operation moved by 1% of the time
where the time goes in v7:
time: 83.6 us; the launch traced here: 83.3 us
  Pallas kernels  82.7 us (99%)
    pallas_call x1, Pallas kernels, on_device(): pl.pallas_call(whole_kernel, out_shape=(grad, grad, piece, piece, piece,...  80.1 us
    pallas_call x1, Pallas kernels, on_device(): pl.pallas_call(hand_kernel, out_shape=(grad, grad, piece, piece, piece, j...  2.62 us

profile of v7, /device:TPU:0, one launch (start us, length us, event | category | flops | bytes accessed | tf_op | source)
XLA Modules:
  0.0 83.3 jit_solution(7201489698109061672)
XLA Ops:
  0.6 80.1 %shard_map.126 = (f32[512,512]{1,0:T(8,128)}, f32[512,512]{1,0:T(8,128)}, f32[64,512]{1,0:T(8,128)}, f32[64,512]{1,0:T(8,128)}, f32[64,512]{1,0:T(8,128)}, /*index=5*/f32[32,512]{1,0:T(8,128)}) custom-call(bf16[512,2048]{1,0:T(8,128)(2,1)} %feat_hbm.1, bf16[4096,512]{1,0:T(8,128)(2,1)} %wv_hbm.1, bf16[4096,512]{1,0:T(8,128)(2,1)} %wg_hbm.1, ...), custom_call_target="tpu_custom_call" | custom-call | tf_op jit(solution)/shard_map/pallas_call | solution.py:916
  80.7 2.6 %shard_map.127 = (f32[512,512]{1,0:T(8,128)}, f32[512,512]{1,0:T(8,128)}, f32[64,512]{1,0:T(8,128)}, f32[64,512]{1,0:T(8,128)}, f32[64,512]{1,0:T(8,128)}, /*index=5*/f32[31,512]{1,0:T(8,128)}, f32[1,512]{1,0:T(1,128)}) custom-call(f32[512,512]{1,0:T(8,128)} %get-tuple-element.20.vgrad, f32[512,512]{1,0:T(8,128)} %get-tuple-element.21.ggrad, ...), custom_call_target="tpu_custom_call" | custom-call | tf_op jit(solution)/shard_map/pallas_call | solution.py:964
